TPU v7x, 32 devices: a whole 2x2x4 slice. The times are simulated.
32 devices in a mesh: sp: 4 (over x, core), tp: 8 (over z, y).
Axes of the slice: x: 2, y: 2, z: 4, core: 2. Of those that a mesh axis runs over, the one named last changes fastest.
Arguments:
- latent: bfloat16 [512, 4096], P('sp', 'tp'), may hold values from -60 to 60
- context: bfloat16 [64, 4096], P('sp', 'tp'), may hold values from -6 to 6
- conditioning: bfloat16 [4096], P('sp'), may hold values from -6 to 6
- context_prompt_vector: bfloat16 [4096], P('sp'), may hold values from -6 to 6
- shift_matrix: bfloat16 [4096, 4096], P('tp', 'sp'), may hold values from -0.09375 to 0.09375
- scale_matrix: bfloat16 [4096, 4096], P('tp', 'sp'), may hold values from -0.09375 to 0.09375
- residual_gate_matrix: bfloat16 [4096, 4096], P('tp', 'sp'), may hold values from -0.09375 to 0.09375
- query_matrix: bfloat16 [2048, 4096], P('tp'), may hold values from -0.09375 to 0.09375
- key_matrix: bfloat16 [2048, 4096], P('tp'), may hold values from -0.09375 to 0.09375
- value_matrix: bfloat16 [4096, 4096], P('tp'), may hold values from -0.09375 to 0.09375
- gate_matrix: bfloat16 [4096, 4096], P('tp'), may hold values from -0.09375 to 0.09375
- decay_down_factor: bfloat16 [2, 4096, 16], replicated, may hold values from -0.09375 to 0.09375
- decay_up_factor: bfloat16 [2, 16, 2048], replicated, may hold values from -1.5 to 1.5
- decay_key_bias: float32 [2, 2048], replicated, may hold values from -0.5 to 7
- spike_log_decay: float32 [2, 512, 16], P(None, 'sp'), may hold values from -2.8 to 0
- output_gain: float32 [4096], P('tp'), may hold values from 0.1 to 1.9
- output_matrix: bfloat16 [4096, 4096], P('tp'), may hold values from -0.375 to 0.375
Outputs:
- mixed: bfloat16 [512, 4096], P('sp', 'tp')
All inputs are finite; a program needn't handle non-finite values.
Results may differ from a plain program's by a relative error of at most 0.013.
Values may be sent and summed in bfloat16 or wider, within the bound.
A program may use at most 64 MiB of HBM per device.

v0:
```python
import functools
import math

import jax
import jax.numpy as jnp
from jax import lax
from jax.experimental import pallas as pl
from jax.experimental.pallas import tpu as pltpu
from jax.sharding import PartitionSpec as P

D = 4096
HEADS = 16
DK = 128
DECAY_RANK = 16
BLK = 64
VGROUP = 64
MESH = pl.DeviceIdType.MESH


epsilon = 1e-05
gate_norm = 16.0
precise = lax.Precision.HIGHEST


def for_sending(value):

    def short(part):
        return part.astype(jnp.bfloat16) if part.dtype == jnp.float32 else part

    return jax.tree.map(short, value)


def from_partner(value, axis, distance):
    return lax.ppermute(value, axis, [(i, i ^ 1 << distance) for i in range(lax.axis_size(axis))])


def carried_in(value, axis, combine, identity, reverse):
    peers, index = (lax.axis_size(axis), lax.axis_index(axis))
    everything = jax.tree.map(
        lambda part, kind: lax.all_gather(part.astype(kind), axis),
        value,
        (jnp.bfloat16, jnp.bfloat16),
    )
    start = jax.tree.map(
        lambda part, zero: jnp.broadcast_to(jnp.asarray(zero, part.dtype), part.shape),
        value,
        identity,
    )

    def turn(k, before):
        at = peers - 1 - k if reverse else k
        reached = at > index if reverse else at < index
        new = combine(
            before, jax.tree.map(lambda part, own: part[at].astype(own.dtype), everything, value)
        )
        return jax.tree.map(lambda a, b: jnp.where(reached, a, b), new, before)

    return lax.fori_loop(0, peers, turn, start)


def linear(rows, weight):
    return lax.dot_general(
        rows, weight, (((1,), (1,)), ((), ())), preferred_element_type=jnp.float32
    )


def modulated(rows, row_sum, row_squares, shift_vec, scale_vec):
    rows_f = rows.astype(jnp.float32)
    mean_val = row_sum / D
    variance = row_squares / D - mean_val * mean_val
    return (
        (rows_f - mean_val) * lax.rsqrt(variance + epsilon) * (1.0 + scale_vec) + shift_vec
    ).astype(jnp.bfloat16)


def reverse_rows(array):
    return jnp.flip(array, axis=0)


def end_state(key_rows, value_rows, log_decay):
    cumulative = jnp.cumsum(log_decay, axis=0)
    totals = cumulative[-1]
    weighted = key_rows * jnp.exp(totals - cumulative)
    return (jnp.exp(totals), jnp.einsum("nhd,nhe->hde", weighted, value_rows, precision=precise))


def combine(earlier, later):
    return (earlier[0] * later[0], later[0][..., None] * earlier[1] + later[1])


def blockwise(queries, key_rows, value_rows, log_decay, carried, block_len):
    length, head_count, _ = queries.shape
    value_width = value_rows.shape[-1]
    blocks = length // block_len

    def shaped(array):
        return array.reshape(blocks, block_len, head_count, array.shape[-1])

    triangle = jnp.tril(jnp.ones((block_len, block_len), jnp.float32))

    def advance(state_now, inputs):
        block_q, block_k, block_v, block_a = inputs
        cumulative = jnp.cumsum(block_a, axis=0)
        block_end = cumulative[-1]
        query_dec = block_q * jnp.exp(cumulative)
        scores = (
            jnp.einsum("ihd,jhd->hij", query_dec, block_k * jnp.exp(-cumulative), precision=precise)
            * triangle
        )
        result = jnp.einsum("hij,jhe->ihe", scores, block_v, precision=precise)
        result = result + jnp.einsum("ihd,hde->ihe", query_dec, state_now, precision=precise)
        state_next = state_now * jnp.exp(block_end)[:, :, None] + jnp.einsum(
            "jhd,jhe->hde", block_k * jnp.exp(block_end - cumulative), block_v, precision=precise
        )
        return (state_next, result)

    _, outputs = lax.scan(
        advance, carried, (shaped(queries), shaped(key_rows), shaped(value_rows), shaped(log_decay))
    )
    return outputs.reshape(length, head_count, value_width)


def head_channels(pieces, per_head, tp_index):
    for bit_number in range(per_head.bit_length() - 1):
        partner = from_partner(
            (for_sending(pieces[0]), for_sending(pieces[1]), for_sending(pieces[2])),
            "tp",
            bit_number,
        )
        upper = tp_index // (1 << bit_number) % 2 == 1
        pieces = tuple(
            (
                jnp.where(
                    upper,
                    jnp.concatenate([theirs, mine], axis=1),
                    jnp.concatenate([mine, theirs], axis=1),
                )
                for mine, theirs in zip(pieces, partner)
            )
        )
    return pieces


def context_totals(fwd_growth, fwd_state, bwd_growth, bwd_state, identity):

    def absorb(carried, piece):
        return (combine(carried, piece), None)

    total_fwd, _ = lax.scan(absorb, identity, (fwd_growth, fwd_state))
    total_bwd, _ = lax.scan(absorb, identity, (bwd_growth, bwd_state), reverse=True)
    return (total_fwd, total_bwd)


def stored(array):
    return lax.optimization_barrier(array.astype(jnp.bfloat16))


def local(
    latent,
    context,
    conditioning,
    context_prompt_vector,
    shift_matrix,
    scale_matrix,
    residual_gate_matrix,
    query_matrix,
    key_matrix,
    value_matrix,
    gate_matrix,
    decay_down_factor,
    decay_up_factor,
    decay_key_bias,
    spike_log_decay,
    output_gain,
    output_matrix,
):
    tp_count = lax.axis_size("tp")
    tp_index = lax.axis_index("tp")
    per_head = max(tp_count // HEADS, 1)
    heads_per_shard = max(HEADS // tp_count, 1)
    leading_head = tp_index // per_head * heads_per_shard
    tok_rows = latent.shape[0]
    conds = jax.nn.silu(
        jnp.stack([conditioning, context_prompt_vector]).astype(jnp.float32)
    ).astype(jnp.bfloat16)
    shifts, scales, gates = lax.psum(
        (
            linear(conds, shift_matrix),
            linear(conds, scale_matrix),
            linear(conds, residual_gate_matrix),
        ),
        "sp",
    )
    down_both = jnp.concatenate([decay_down_factor[0].T, decay_down_factor[1].T], axis=0)
    lat_weights = (query_matrix, key_matrix, value_matrix, gate_matrix, down_both)
    ctx_weights = (key_matrix, value_matrix, down_both)
    lat_f = latent.astype(jnp.float32)
    ctx_f = context.astype(jnp.float32)
    lat_sum, lat_squares, ctx_sum, ctx_squares = lax.psum(
        (
            jnp.sum(lat_f, axis=1, keepdims=True),
            jnp.sum(lat_f * lat_f, axis=1, keepdims=True),
            jnp.sum(ctx_f, axis=1, keepdims=True),
            jnp.sum(ctx_f * ctx_f, axis=1, keepdims=True),
        ),
        "tp",
    )
    latent_normalized = modulated(latent, lat_sum, lat_squares, shifts[0], scales[0])
    normed_ctx = modulated(context, ctx_sum, ctx_squares, shifts[1], scales[1])
    lat_piece = lax.all_gather(latent_normalized, "tp", axis=1, tiled=True)
    ctx_piece = lax.all_gather(normed_ctx, "tp", axis=1, tiled=True)
    lat_new = tuple((linear(lat_piece, weight) for weight in lat_weights))
    ctx_new = tuple((linear(ctx_piece, weight) for weight in ctx_weights))
    query_part, key_part, value_part, gate_part, low_rank_part = lat_new
    ctx_key_part, ctx_value_part, ctx_low = ctx_new
    query_full, key_full, ctx_key_full = head_channels(
        (stored(query_part), stored(key_part), stored(ctx_key_part)), per_head, tp_index
    )

    def split_heads(rows, width):
        return rows.astype(jnp.float32).reshape(rows.shape[0], heads_per_shard, width)

    value_cols = value_part.shape[1] // heads_per_shard
    queries = split_heads(query_full, DK) * DK ** (-0.5)
    key_rows = split_heads(key_full, DK)
    ctx_keys = split_heads(ctx_key_full, DK)
    values_lat = split_heads(stored(value_part), value_cols)
    values_ctx = split_heads(stored(ctx_value_part), value_cols)
    gate_rows = stored(gate_part).astype(jnp.float32)

    def per_head_decay(low_rows, direction):
        up_part = lax.dynamic_slice_in_dim(
            decay_up_factor[direction], leading_head * DK, heads_per_shard * DK, 1
        ).astype(jnp.float32)
        bias_part = lax.dynamic_slice_in_dim(
            decay_key_bias[direction], leading_head * DK, heads_per_shard * DK, 0
        )
        pre_act = jnp.dot(low_rows, up_part, precision=precise) + bias_part
        return (jax.nn.log_sigmoid(pre_act) / gate_norm).reshape(
            low_rows.shape[0], heads_per_shard, DK
        )

    decay_spikes = lax.dynamic_slice_in_dim(spike_log_decay, leading_head, heads_per_shard, 2)
    latent_forward = per_head_decay(low_rank_part[:, :DECAY_RANK], 0) + decay_spikes[0][:, :, None]
    latent_backward = per_head_decay(low_rank_part[:, DECAY_RANK:], 1) + decay_spikes[1][:, :, None]
    ctx_fwd = per_head_decay(ctx_low[:, :DECAY_RANK], 0)
    ctx_bwd = per_head_decay(ctx_low[:, DECAY_RANK:], 1)
    cf_growth, cf_state = end_state(ctx_keys, values_ctx, ctx_fwd)
    cb_growth, cb_state = end_state(
        reverse_rows(ctx_keys), reverse_rows(values_ctx), reverse_rows(ctx_bwd)
    )
    lf_growth, lf_state = end_state(key_rows, values_lat, latent_forward)
    lb_growth, lb_state = end_state(
        reverse_rows(key_rows), reverse_rows(values_lat), reverse_rows(latent_backward)
    )
    identity = (
        jnp.ones((heads_per_shard, DK), jnp.float32),
        jnp.zeros((heads_per_shard, DK, value_cols), jnp.float32),
    )
    ctx_gathered = (
        lax.all_gather(cf_growth[None].astype(jnp.bfloat16), "sp", axis=0, tiled=True).astype(
            jnp.float32
        ),
        lax.all_gather(cf_state[None].astype(jnp.bfloat16), "sp", axis=0, tiled=True).astype(
            jnp.float32
        ),
        lax.all_gather(cb_growth[None].astype(jnp.bfloat16), "sp", axis=0, tiled=True).astype(
            jnp.float32
        ),
        lax.all_gather(cb_state[None].astype(jnp.bfloat16), "sp", axis=0, tiled=True).astype(
            jnp.float32
        ),
    )
    total_fwd, total_bwd = context_totals(
        ctx_gathered[0], ctx_gathered[1], ctx_gathered[2], ctx_gathered[3], identity
    )
    prefix = carried_in((lf_growth, lf_state), "sp", combine, identity, False)
    suffix = carried_in((lb_growth, lb_state), "sp", combine, identity, True)
    start_fwd = combine(total_fwd, prefix)[1]
    start_bwd = combine(total_bwd, suffix)[1]
    zero_state = jnp.zeros((heads_per_shard, DK, value_cols), jnp.float32)

    def direction_out(query_rows, key_list, value_list, log_decay, start_state):
        local_part = blockwise(query_rows, key_list, value_list, log_decay, zero_state, BLK)
        reach = query_rows * jnp.exp(jnp.cumsum(log_decay, axis=0))
        return local_part + jnp.einsum("nhd,hde->nhe", reach, start_state, precision=precise)

    out_fwd = direction_out(queries, key_rows, values_lat, latent_forward, start_fwd)
    out_bwd = reverse_rows(
        direction_out(
            reverse_rows(queries),
            reverse_rows(key_rows),
            reverse_rows(values_lat),
            reverse_rows(latent_backward),
            start_bwd,
        )
    )
    grouped = (out_fwd + out_bwd).reshape(tok_rows, -1, VGROUP)
    grouped = grouped * lax.rsqrt(jnp.mean(grouped * grouped, axis=-1, keepdims=True) + epsilon)
    heads_out = (grouped.reshape(tok_rows, -1) * output_gain * jax.nn.silu(gate_rows)).astype(
        jnp.bfloat16
    )
    branch = linear(lax.all_gather(heads_out, "tp", axis=1, tiled=True), output_matrix)
    return (latent.astype(jnp.float32) + gates[0] * branch).astype(jnp.bfloat16)


def exact(a, b):
    return lax.dot_general(
        a, b, (((1,), (0,)), ((), ())), precision=precise, preferred_element_type=jnp.float32
    )


def nt(a, b):
    return lax.dot_general(a, b, (((1,), (1,)), ((), ())), preferred_element_type=jnp.float32)


def nn(a, b):
    return lax.dot_general(a, b, (((1,), (0,)), ((), ())), preferred_element_type=jnp.float32)


def tn(a, b):
    return lax.dot_general(a, b, (((0,), (0,)), ((), ())), preferred_element_type=jnp.float32)


def short(value):
    return value.astype(jnp.bfloat16)


def log_decay_of(low, up, bias):
    pre = exact(low, up) + bias
    return (jnp.minimum(pre, 0.0) - jnp.log1p(jnp.exp(-jnp.abs(pre)))) / gate_norm


def triangle_of(size, upper):
    i = lax.broadcasted_iota(jnp.int32, (size, size), 0)
    j = lax.broadcasted_iota(jnp.int32, (size, size), 1)
    return (j >= i) if upper else (j <= i)


def layer_kernel(
    n,
    s,
    inner,
    rows,
    crows,
    feats,
    heads,
    dv,
    latent,
    context,
    conditioning,
    prompt,
    shift_m,
    scale_m,
    gate_m,
    query_m,
    key_m,
    value_m,
    og_m,
    down,
    up,
    bias,
    spike,
    gain,
    out_m,
    out_ref,
    x_all,
    xn,
    acc,
    low_acc,
    mod_w,
    proj_w,
    out_w,
    down_v,
    up_v,
    bias_v,
    spike_v,
    gain_v,
    cond_v,
    mod_own,
    mod_recv,
    mod_all,
    proj,
    ctx_kv,
    ctx_low,
    tot_own,
    tot_recv,
    st_own,
    st_recv,
    local_out,
    ho_all,
    load_sem,
    xs_up,
    xr_up,
    xs_dn,
    xr_dn,
    xs_y,
    xr_y,
    m1_s,
    m1_r,
    m2_s,
    m2_r,
    kv_s,
    kv_r,
    lo_s,
    lo_r,
    to_s,
    to_r,
    st_s,
    st_r,
    hs_up,
    hr_up,
    hs_dn,
    hr_dn,
    hs_y,
    hr_y,
):
    me = lax.axis_index("tp")
    sp = lax.axis_index("sp")
    hk = heads * DK
    hv = heads * dv
    model = n * feats
    mine = pl.ds(pl.multiple_of(me * feats, feats), feats)

    loads = []

    def load(src, dst):
        copy = pltpu.make_async_copy(src, dst, load_sem.at[len(loads)])
        loads.append(copy)
        copy.start()
        return copy

    first = [
        load(conditioning, cond_v.at[0]),
        load(prompt, cond_v.at[1]),
        load(shift_m, mod_w.at[0]),
        load(scale_m, mod_w.at[1]),
        load(gate_m, mod_w.at[2]),
    ]
    own_x = [
        load(latent, x_all.at[pl.ds(0, rows), mine]),
        load(context, x_all.at[pl.ds(rows, crows), mine]),
    ]
    weights = [
        load(query_m, proj_w.at[pl.ds(0, hk)]),
        load(key_m, proj_w.at[pl.ds(hk, hk)]),
        load(value_m, proj_w.at[pl.ds(2 * hk, hv)]),
        load(og_m, proj_w.at[pl.ds(2 * hk + hv, hv)]),
        load(down, down_v),
    ]
    head_cols = pl.ds(pl.multiple_of(me * hk, hk), hk)
    small = [
        load(up.at[:, :, head_cols], up_v),
        load(bias.at[:, head_cols], bias_v),
        load(spike, spike_v),
        load(gain, gain_v),
    ]
    last = load(out_m, out_w)

    barrier = pltpu.get_barrier_semaphore()
    for d in range(1, n):
        pl.semaphore_signal(
            barrier, inc=1, device_id={"tp": lax.rem(me + d, n)}, device_id_type=MESH
        )
    for d in range(1, s):
        pl.semaphore_signal(
            barrier, inc=1, device_id={"sp": lax.rem(sp + d, s)}, device_id_type=MESH
        )
    pl.semaphore_wait(barrier, n - 1 + s - 1)

    started = []

    def send(src, dst, send_sem, recv_sem, axis, d):
        index, count = (me, n) if axis == "tp" else (sp, s)
        copy = pltpu.make_async_remote_copy(
            src_ref=src,
            dst_ref=dst,
            send_sem=send_sem.at[d - 1],
            recv_sem=recv_sem.at[d - 1],
            device_id={axis: lax.rem(index + d, count)},
            device_id_type=MESH,
        )
        copy.start()
        started.append(copy)
        return copy

    line = n // inner
    z, y = lax.div(me, inner), lax.rem(me, inner)

    def block_of(at, column):
        return at * inner + column

    class Gather:
        def __init__(self, view, pieces, up, down, across):
            self.view, self.pieces = view, pieces
            self.lanes = {"up": up, "down": down, "across": across}

        def copy(self, lane, block, piece, slot, target):
            sends, recvs = self.lanes[lane]
            ref = self.view(block, piece)
            return pltpu.make_async_remote_copy(
                src_ref=ref,
                dst_ref=ref,
                send_sem=sends.at[slot, piece],
                recv_sem=recvs.at[slot, piece],
                device_id={"tp": target},
                device_id_type=MESH,
            )

        def hop(self, lane, at, piece, slot):
            target = {
                "up": block_of(jnp.minimum(z + 1, line - 1), y),
                "down": block_of(jnp.maximum(z - 1, 0), y),
                "across": block_of(z, inner - 1 - y),
            }[lane]
            return self.copy(lane, block_of(at, y), piece, slot, target)

        def sends(self, k, piece, act):
            for lane, at, has, onward, slot in (
                ("up", z - k, z >= k, z + 1 < line, max(2 * k - 1, 0)),
                ("down", z + k, z + k < line, z > 0, 2 * k),
            ):
                if k < line - 1:
                    pl.when(has & onward)(lambda: act(self.hop(lane, at, piece, k)))
                if inner > 1 and (k > 0 or lane == "up"):
                    pl.when(has)(lambda: act(self.hop("across", at, piece, slot)))

        def start(self):
            for piece in range(self.pieces):
                self.sends(0, piece, lambda c: c.start())

        def step(self, k):
            for piece in range(self.pieces):
                for lane, at, has in (("up", z - k, z >= k), ("down", z + k, z + k < line)):
                    pl.when(has)(lambda: self.hop(lane, at, piece, k - 1).wait_recv())
                self.sends(k, piece, lambda c: c.start())

        def column(self, k, work):
            pl.when(z >= k)(lambda: work(block_of(z - k, y)))
            pl.when(z + k < line)(lambda: work(block_of(z + k, y)))

        def other(self, k, work):
            if inner == 1:
                return

            def arrive(at, slot):
                block = block_of(at, inner - 1 - y)
                for piece in range(self.pieces):
                    self.copy("across", block, piece, slot, block).wait_recv()
                work(block)

            if k == 0:
                arrive(z, 0)
                return
            pl.when(z >= k)(lambda: arrive(z - k, 2 * k - 1))
            pl.when(z + k < line)(lambda: arrive(z + k, 2 * k))

        def drain(self):
            for k in range(line):
                for piece in range(self.pieces):
                    self.sends(k, piece, lambda c: c.wait_send())

    both = rows + crows
    cut = both // 32 * 16

    def x_view(block, piece):
        part = pl.ds(0, cut) if piece == 0 else pl.ds(cut, both - cut)
        return x_all.at[part, pl.ds(pl.multiple_of(block * feats, feats), feats)]

    xg = Gather(x_view, 2, (xs_up, xr_up), (xs_dn, xr_dn), (xs_y, xr_y))
    for copy in own_x:
        copy.wait()
    xg.start()

    for copy in first:
        copy.wait()
    def one_row(which):
        part = cond_v[which].astype(jnp.float32)
        return jnp.concatenate([part[r : r + 1] for r in range(part.shape[0])], axis=1)

    row_of = lax.broadcasted_iota(jnp.int32, (16, shift_m.shape[1]), 0)
    conds = jnp.where(row_of == 0, one_row(0), one_row(1))
    conds = short(conds * lax.logistic(conds))
    for which in range(3):
        mod_own[2 * which : 2 * which + 2, :] = nt(conds, mod_w[which])[0:2]
    mod_own[6:8, :] = jnp.zeros((2, feats), jnp.float32)
    m1 = {
        d: send(mod_own, mod_recv.at[d - 1], m1_s, m1_r, "sp", d) for d in range(1, s)
    }

    own = x_all[:, mine]
    ones = jnp.ones((16, feats), jnp.bfloat16)
    own_f = own.astype(jnp.float32)
    rest = own_f * own_f
    row_squares = jnp.zeros((16, both), jnp.float32)
    for _ in range(3):
        top = short(rest)
        row_squares = row_squares + nt(ones, top)
        rest = rest - top.astype(jnp.float32)
    row_sum = nt(ones, own)

    if line > 1:
        xg.step(1)
    for d in range(1, s):
        m1[d].wait_recv()
    total = mod_own[...]
    for d in range(1, s):
        total = total + mod_recv[d - 1]
    mod_all[:, mine] = total
    stat_cols = pl.ds(pl.multiple_of(me * feats, feats), both)
    mod_all[6:7, stat_cols] = row_sum[0:1]
    mod_all[7:8, stat_cols] = row_squares[0:1]
    m2 = {
        d: send(mod_all.at[:, mine], mod_all.at[:, mine], m2_s, m2_r, "tp", d)
        for d in range(1, n)
    }
    tile = math.gcd(2 * hk + 2 * hv, 512)
    columns = acc.shape[1]
    acc[...] = jnp.zeros(acc.shape, jnp.float32)
    low_acc[...] = jnp.zeros(low_acc.shape, jnp.float32)

    def moments():
        for d in range(1, n):
            m2[d].wait_recv()
        diagonal = lax.broadcasted_iota(jnp.int32, (both, both), 0) == lax.broadcasted_iota(
            jnp.int32, (both, both), 1
        )

        def column_of(row):
            whole_row = sum(mod_all[row : row + 1, b * feats : b * feats + both] for b in range(n))
            return jnp.sum(jnp.where(diagonal, whole_row, 0.0), axis=1, keepdims=True) / model

        mean = column_of(6)
        return mean, lax.rsqrt(column_of(7) - mean * mean + epsilon)

    def project_block(block, mean, spread):
        cols = pl.ds(pl.multiple_of(block * feats, feats), feats)
        x = (x_all[:, cols].astype(jnp.float32) - mean) * spread
        mod = mod_all[:, cols]
        xn[0:rows, :] = short(x[0:rows] * (1.0 + mod[2:3]) + mod[0:1])
        xn[rows:, :] = short(x[rows:] * (1.0 + mod[3:4]) + mod[1:2])
        low_acc[...] += nt(xn[...], down_v[:, cols])

        for t in range(columns // tile):
            out = slice(t * tile, (t + 1) * tile)
            acc[:, out] += nt(xn[...], proj_w[out, cols])

    ready = None
    for k in range(2, line + 1):
        if k < line:
            xg.step(k)
        if ready is None:
            ready = moments()
            for copy in weights:
                copy.wait()
            work = lambda block: project_block(block, *ready)
            work(me)
        xg.column(k - 1, work)
        xg.other(k - 2, work)
    xg.other(line - 1, work)
    proj[...] = short(acc[...])

    own_ctx = pl.ds(pl.multiple_of(sp * crows, crows), crows)
    ctx_kv[own_ctx, :] = proj[rows:, hk : 2 * hk + hv]
    ctx_low[own_ctx, :] = jnp.zeros((crows, ctx_low.shape[1]), jnp.float32)
    ctx_low[own_ctx, 0 : 2 * DECAY_RANK] = low_acc[rows:]
    kv = {
        d: send(ctx_kv.at[own_ctx], ctx_kv.at[own_ctx], kv_s, kv_r, "sp", d)
        for d in range(1, s)
    }
    lo = {
        d: send(ctx_low.at[own_ctx], ctx_low.at[own_ctx], lo_s, lo_r, "sp", d)
        for d in range(1, s)
    }

    for copy in small:
        copy.wait()
    slot_head = lax.broadcasted_iota(jnp.int32, (spike_v.shape[1], hk), 0)
    lane_head = lax.broadcasted_iota(jnp.int32, (spike_v.shape[1], hk), 1) // DK
    pick = jnp.where(slot_head == me * heads + lane_head, 1.0, 0.0)
    none = jnp.zeros((DECAY_RANK, hk), jnp.float32)
    ups = [
        jnp.concatenate([up_v[0].astype(jnp.float32), none], axis=0),
        jnp.concatenate([none, up_v[1].astype(jnp.float32)], axis=0),
    ]
    cum = []
    for direction in range(2):
        logs = log_decay_of(low_acc[0:rows], ups[direction], bias_v[direction : direction + 1])
        logs = logs + lax.dot_general(
            spike_v[direction],
            pick,
            (((0,), (0,)), ((), ())),
            precision=precise,
            preferred_element_type=jnp.float32,
        )
        cum.append(exact(triangle_of(rows, direction == 1).astype(jnp.float32), logs))
    whole = [cum[0][rows - 1 : rows], cum[1][0:1]]
    tot_own[0:1, :] = whole[0]
    tot_own[1:2, :] = whole[1]
    tot_own[2:8, :] = jnp.zeros((6, hk), jnp.float32)
    to = {d: send(tot_own, tot_recv.at[d - 1], to_s, to_r, "sp", d) for d in range(1, s)}

    keys = proj[0:rows, hk : 2 * hk].astype(jnp.float32)
    for direction in range(2):
        weighted = short(keys * jnp.exp(whole[direction] - cum[direction]))
        for h in range(heads):
            st_own[direction, h * DK : (h + 1) * DK, :] = short(
                tn(
                    weighted[:, h * DK : (h + 1) * DK],
                    proj[0:rows, 2 * hk + h * dv : 2 * hk + (h + 1) * dv],
                )
            )
    st = {}
    for d in range(1, s):
        later = lax.rem(sp + d, s) > sp
        st[d] = send(
            st_own.at[jnp.where(later, 0, 1)], st_recv.at[d - 1], st_s, st_r, "sp", d
        )

    queries = proj[0:rows, 0:hk].astype(jnp.float32) * DK ** (-0.5)
    blocks = rows // BLK

    def span(b):
        return slice(b * BLK, (b + 1) * BLK)

    inside = [[], []]
    for b in range(blocks):
        f = cum[0][span(b)]
        inside[0].append(f if b == 0 else f - cum[0][b * BLK - 1 : b * BLK])
        f = cum[1][span(b)]
        inside[1].append(
            f if b == blocks - 1 else f - cum[1][(b + 1) * BLK : (b + 1) * BLK + 1]
        )
    ends = [[part[BLK - 1 : BLK] for part in inside[0]], [part[0:1] for part in inside[1]]]
    q_dec = [[short(queries[span(b)] * jnp.exp(inside[e][b])) for b in range(blocks)] for e in range(2)]
    k_dec = [[short(keys[span(b)] * jnp.exp(-inside[e][b])) for b in range(blocks)] for e in range(2)]
    k_end = [
        [short(keys[span(b)] * jnp.exp(ends[e][b] - inside[e][b])) for b in range(blocks)]
        for e in range(2)
    ]
    lower, upper = triangle_of(BLK, False), triangle_of(BLK, True)
    for h in range(heads):
        ch = slice(h * DK, (h + 1) * DK)
        lines = []
        for b in range(blocks):
            strip = []
            for c in range(blocks):
                if b == c:
                    strip.append(
                        jnp.where(lower, nt(q_dec[0][b][:, ch], k_dec[0][b][:, ch]), 0.0)
                        + jnp.where(upper, nt(q_dec[1][b][:, ch], k_dec[1][b][:, ch]), 0.0)
                    )
                    continue
                e = 0 if c < b else 1
                near = q_dec[e][b][:, ch]
                between = range(c + 1, b) if c < b else range(b + 1, c)
                if len(between) > 0:
                    gap = sum(ends[e][m][:, ch] for m in between)
                    near = short(queries[span(b)][:, ch] * jnp.exp(inside[e][b][:, ch] + gap))
                strip.append(nt(near, k_end[e][c][:, ch]))
            lines.append(jnp.concatenate(strip, axis=1) if blocks > 1 else strip[0])
        scores = short(jnp.concatenate(lines, axis=0) if blocks > 1 else lines[0])
        local_out[:, h * dv : (h + 1) * dv] = nn(
            scores, proj[0:rows, 2 * hk + h * dv : 2 * hk + (h + 1) * dv]
        )

    for d in range(1, s):
        kv[d].wait_recv()
        lo[d].wait_recv()
    ctx_keys = ctx_kv[:, 0:hk].astype(jnp.float32)
    ctx_states = []
    for direction in range(2):
        logs = log_decay_of(
            ctx_low[:, 0 : 2 * DECAY_RANK],
            ups[direction],
            bias_v[direction : direction + 1],
        )
        length = s * crows
        c = exact(triangle_of(length, direction == 1).astype(jnp.float32), logs)
        end = c[length - 1 : length] if direction == 0 else c[0:1]
        weighted = short(ctx_keys * jnp.exp(end - c))
        ctx_states.append(
            [
                short(
                    tn(
                        weighted[:, h * DK : (h + 1) * DK],
                        ctx_kv[:, hk + h * dv : hk + (h + 1) * dv],
                    )
                )
                for h in range(heads)
            ]
        )

    for d in range(1, s):
        to[d].wait_recv()
    places = {d: lax.rem(sp - d + s, s) for d in range(1, s)}

    def passed(low_end, high_end, direction):
        result = jnp.zeros((1, hk), jnp.float32)
        for d in range(1, s):
            held = jnp.where((places[d] > low_end) & (places[d] < high_end), 1.0, 0.0)
            result = result + held * tot_recv[d - 1][direction : direction + 1]
        return result

    ctx_reach = [
        short(queries * jnp.exp(cum[0] + passed(-1, sp, 0))),
        short(queries * jnp.exp(cum[1] + passed(sp, s, 1))),
    ]
    for h in range(heads):
        ch = slice(h * DK, (h + 1) * DK)
        local_out[:, h * dv : (h + 1) * dv] += nn(
            jnp.concatenate([r[:, ch] for r in ctx_reach], axis=1),
            jnp.concatenate([ctx_states[e][h] for e in range(2)], axis=0),
        )
    reach = []
    for d in range(1, s):
        p = places[d]
        before = jnp.where(p < sp, 1.0, 0.0)
        exponent = before * (cum[0] + passed(p, sp, 0)) + (1.0 - before) * (
            cum[1] + passed(sp, p, 1)
        )
        reach.append(short(queries * jnp.exp(exponent)))
    gate_rows = proj[0:rows, 2 * hk + hv :].astype(jnp.float32)
    small_gate = gate_rows * lax.logistic(gate_rows) * gain_v[...]
    gi = lax.broadcasted_iota(jnp.int32, (dv, dv), 0) // VGROUP
    gj = lax.broadcasted_iota(jnp.int32, (dv, dv), 1) // VGROUP
    group = jnp.where(gi == gj, 1.0, 0.0).astype(jnp.bfloat16)
    for d in range(1, s):
        st[d].wait_recv()
    for h in range(heads):
        ch = slice(h * DK, (h + 1) * DK)
        vc = slice(h * dv, (h + 1) * dv)
        o = local_out[:, vc]
        for d in range(1, s):
            o = o + nn(reach[d - 1][:, ch], st_recv[d - 1, ch, :])
        squares = o * o
        top = short(squares)
        rest = short(squares - top.astype(jnp.float32))
        power = (nn(top, group) + nn(rest, group)) * (1.0 / VGROUP)
        ho_all[me, :, vc] = short(o * lax.rsqrt(power + epsilon) * small_gate[:, vc])

    def ho_view(block, piece):
        return ho_all.at[block, pl.ds(piece * (rows // 4), rows // 4)]

    hg = Gather(ho_view, 4, (hs_up, hr_up), (hs_dn, hr_dn), (hs_y, hr_y))
    hg.start()
    last.wait()
    local_out[...] = nt(ho_all[me], out_w[:, mine])

    def add_block(block):
        cols = pl.ds(pl.multiple_of(block * feats, feats), feats)
        local_out[...] += nt(ho_all[block], out_w[:, cols])

    for k in range(1, line):
        hg.step(k)
        hg.other(k - 1, add_block)
        hg.column(k, add_block)
    hg.other(line - 1, add_block)
    gates = mod_all[:, mine][4:5]
    out_ref[...] = short(x_all[0:rows, mine].astype(jnp.float32) + gates * local_out[...])
    for copy in started:
        copy.wait_send()
    xg.drain()
    hg.drain()


def one_kernel(
    latent,
    context,
    conditioning,
    context_prompt_vector,
    shift_matrix,
    scale_matrix,
    residual_gate_matrix,
    query_matrix,
    key_matrix,
    value_matrix,
    gate_matrix,
    decay_down_factor,
    decay_up_factor,
    decay_key_bias,
    spike_log_decay,
    output_gain,
    output_matrix,
):
    n, s = lax.axis_size("tp"), lax.axis_size("sp")
    rows, feats = latent.shape
    crows = context.shape[0]
    heads = HEADS // n
    hk, hv = query_matrix.shape[0], value_matrix.shape[0]
    dv = hv // heads
    model = n * feats
    both = rows + crows
    inputs = conditioning.shape[0]
    bf, f32 = jnp.bfloat16, jnp.float32
    vmem, dma = pltpu.VMEM, pltpu.SemaphoreType.DMA
    pair = lambda k: [dma((k,)), dma((k,))]
    scratch = [
        vmem((both, model), bf),
        vmem((both, feats), bf),
        vmem((both, 2 * hk + 2 * hv), f32),
        vmem((both, 2 * DECAY_RANK), f32),
        vmem((3, feats, inputs), bf),
        vmem((2 * hk + 2 * hv, model), bf),
        vmem((output_matrix.shape[0], model), bf),
        vmem((2 * DECAY_RANK, model), bf),
        vmem((2, DECAY_RANK, hk), bf),
        vmem((2, hk), f32),
        vmem((2, HEADS, rows), f32),
        vmem((1, hv), f32),
        vmem((2, inputs // 128, 128), bf),
        vmem((8, feats), f32),
        vmem((s - 1, 8, feats), f32),
        vmem((8, model), f32),
        vmem((both, 2 * hk + 2 * hv), bf),
        vmem((s * crows, hk + hv), bf),
        vmem((s * crows, 128), f32),
        vmem((8, hk), f32),
        vmem((s - 1, 8, hk), f32),
        vmem((2, hk, dv), bf),
        vmem((s - 1, hk, dv), bf),
        vmem((rows, hv), f32),
        vmem((n, rows, hv), bf),
        dma((17,)),
    ]
    inner = 2 if n % 2 == 0 else 1
    line = n // inner
    hops = max(line - 1, 1)
    counts = (hops, hops, hops, hops, 2 * line - 1, 2 * line - 1)
    scratch += [dma((k, 2)) for k in counts]
    for count in (s - 1, n - 1, s - 1, s - 1, s - 1, s - 1):
        scratch += pair(count)
    scratch += [dma((k, 4)) for k in counts]
    return pl.pallas_call(
        functools.partial(layer_kernel, n, s, inner, rows, crows, feats, heads, dv),
        out_shape=jax.ShapeDtypeStruct((rows, feats), bf),
        in_specs=[pl.BlockSpec(memory_space=pl.ANY)] * 17,
        out_specs=pl.BlockSpec(memory_space=pltpu.VMEM),
        scratch_shapes=scratch,
        compiler_params=pltpu.CompilerParams(
            collective_id=0, has_side_effects=True, vmem_limit_bytes=60 * 1024 * 1024
        ),
        name="layer",
    )(
        latent,
        context,
        conditioning.reshape(-1, 128),
        context_prompt_vector.reshape(-1, 128),
        shift_matrix,
        scale_matrix,
        residual_gate_matrix,
        query_matrix,
        key_matrix,
        value_matrix,
        gate_matrix,
        jnp.swapaxes(decay_down_factor, 1, 2).reshape(2 * DECAY_RANK, model),
        decay_up_factor,
        decay_key_bias,
        jnp.swapaxes(spike_log_decay, 1, 2),
        output_gain.reshape(1, -1),
        output_matrix,
    )


def solution(mesh):
    placed = (
        P("sp", "tp"),
        P("sp", "tp"),
        P("sp"),
        P("sp"),
        P("tp", "sp"),
        P("tp", "sp"),
        P("tp", "sp"),
        P("tp", None),
        P("tp", None),
        P("tp", None),
        P("tp", None),
        P(),
        P(),
        P(),
        P(None, "sp", None),
        P("tp"),
        P("tp", None),
    )
    whole_heads = HEADS % mesh.shape["tp"] == 0
    return jax.shard_map(
        one_kernel if whole_heads else local, mesh=mesh, in_specs=placed, out_specs=P("sp", "tp"), check_vma=False
    )
```

profile of v0, /device:TPU:0, one launch (start us, length us, event | category | flops | bytes accessed | tf_op | source)
XLA Modules:
  0.0 50.6 jit_solution(3516350239920724735)
XLA Ops:
  0.0 49.0 %layer.1 = bf16[128,512]{1,0:T(8,128)(2,1)} custom-call(bf16[128,512]{1,0:T(8,128)(2,1)} %latent.1, bf16[16,512]{1,0:T(8,128)(2,1)} %context.1, bf16[8,128]{1,0:T(8,128)(2,1)} %bitcast.9, bf16[8,128]{1,0:T(8,128)(2,1)} %bitcast.10, bf16[512,1024]{1,0:T(8,128)(2,1)} %shift_m.1, bf16[512,1024]{1,0:T(8,128)(2,1)} %scale_m.1, bf16[512,1024]{1,0:T(8,128)(2,1)} %gate_m.1, ...), custom_call_target="tpu_custom_call" | custom-call | tf_op jit(solution)/shard_map/layer/pallas_call | solution.py:934
  49.0 1.6 %copy.19 = bf16[128,512]{1,0:T(8,128)(2,1)} copy(bf16[128,512]{1,0:T(8,128)(2,1)} %layer.1) | data formatting | bytes 262144
where the time goes:
time: 50.8 us; the launch traced here: 50.6 us
  Pallas kernels  49 us (96%)
  local copies, waits for them, and re-layouts  1.57 us (3%)
    pallas_call x1, Pallas kernels, one_kernel(): pl.pallas_call(functools.partial(layer_kernel, n, s, inner, rows, crows,...  49 us
    unnamed x1, local copies, waits for them, and re-layouts  1.57 us

commit v1 on v0

--- a/solution.py
+++ b/solution.py
@@ -326,8 +326,14 @@
     return value.astype(jnp.bfloat16)
 
 
-def log_decay_of(low, up, bias):
-    pre = exact(low, up) + bias
+def terms(value):
+    first = short(value)
+    rest = value - first.astype(jnp.float32)
+    second = short(rest)
+    return first, second, short(rest - second.astype(jnp.float32))
+
+
+def log_sigmoid(pre):
     return (jnp.minimum(pre, 0.0) - jnp.log1p(jnp.exp(-jnp.abs(pre)))) / gate_norm
 
 
@@ -346,6 +352,8 @@
     feats,
     heads,
     dv,
+    parts,
+    hparts,
     latent,
     context,
     conditioning,
@@ -380,6 +388,10 @@
     mod_own,
     mod_recv,
     mod_all,
+    gate_own,
+    gate_recv,
+    stat_all,
+    spike_rows,
     proj,
     ctx_kv,
     ctx_low,
@@ -389,17 +401,16 @@
     st_recv,
     local_out,
     ho_all,
+    total_out,
     load_sem,
-    xs_up,
-    xr_up,
-    xs_dn,
-    xr_dn,
-    xs_y,
-    xr_y,
     m1_s,
     m1_r,
     m2_s,
     m2_r,
+    mg_s,
+    mg_r,
+    sa_s,
+    sa_r,
     kv_s,
     kv_r,
     lo_s,
@@ -408,19 +419,17 @@
     to_r,
     st_s,
     st_r,
-    hs_up,
-    hr_up,
-    hs_dn,
-    hr_dn,
-    hs_y,
-    hr_y,
+    *gather_sems,
 ):
     me = lax.axis_index("tp")
     sp = lax.axis_index("sp")
     hk = heads * DK
     hv = heads * dv
     model = n * feats
-    mine = pl.ds(pl.multiple_of(me * feats, feats), feats)
+    both = rows + crows
+    width = feats // parts
+    hwidth = hv // hparts
+    f32 = jnp.float32
 
     loads = []
 
@@ -430,16 +439,28 @@
         copy.start()
         return copy
 
+    own_x = []
+    for p in range(parts):
+        cols = pl.ds(p * width, width)
+        own_x.append(
+            (
+                load(latent.at[:, cols], x_all.at[me * parts + p, pl.ds(0, rows)]),
+                load(context.at[:, cols], x_all.at[me * parts + p, pl.ds(rows, crows)]),
+            )
+        )
     first = [
         load(conditioning, cond_v.at[0]),
         load(prompt, cond_v.at[1]),
         load(shift_m, mod_w.at[0]),
         load(scale_m, mod_w.at[1]),
-        load(gate_m, mod_w.at[2]),
     ]
-    own_x = [
-        load(latent, x_all.at[pl.ds(0, rows), mine]),
-        load(context, x_all.at[pl.ds(rows, crows), mine]),
+    gate_load = load(gate_m, mod_w.at[2])
+    head_cols = pl.ds(pl.multiple_of(me * hk, hk), hk)
+    small = [
+        load(up.at[:, :, head_cols], up_v),
+        load(bias.at[:, head_cols], bias_v),
+        load(spike, spike_v),
+        load(gain, gain_v),
     ]
     weights = [
         load(query_m, proj_w.at[pl.ds(0, hk)]),
@@ -448,13 +469,6 @@
         load(og_m, proj_w.at[pl.ds(2 * hk + hv, hv)]),
         load(down, down_v),
     ]
-    head_cols = pl.ds(pl.multiple_of(me * hk, hk), hk)
-    small = [
-        load(up.at[:, :, head_cols], up_v),
-        load(bias.at[:, head_cols], bias_v),
-        load(spike, spike_v),
-        load(gain, gain_v),
-    ]
     last = load(out_m, out_w)
 
     barrier = pltpu.get_barrier_semaphore()
@@ -475,8 +489,8 @@
         copy = pltpu.make_async_remote_copy(
             src_ref=src,
             dst_ref=dst,
-            send_sem=send_sem.at[d - 1],
-            recv_sem=recv_sem.at[d - 1],
+            send_sem=send_sem,
+            recv_sem=recv_sem,
             device_id={axis: lax.rem(index + d, count)},
             device_id_type=MESH,
         )
@@ -486,18 +500,34 @@
 
     line = n // inner
     z, y = lax.div(me, inner), lax.rem(me, inner)
+    mate = z + 1 - 2 * lax.rem(z, 2)
+    paired = inner > 1 and line % 2 == 0
+    at_end = (z == 0) | (z == line - 1)
+
+    def level(i):
+        table = []
+        for at in range(line):
+            order = [at]
+            for k in range(1, line):
+                order += [b for b in (at - k, at + k) if 0 <= b < line]
+            table.append(order[i])
+        return sum(jnp.where(z == at, table[at], 0) for at in range(line))
 
     def block_of(at, column):
         return at * inner + column
 
     class Gather:
-        def __init__(self, view, pieces, up, down, across):
-            self.view, self.pieces = view, pieces
-            self.lanes = {"up": up, "down": down, "across": across}
+        def __init__(self, ref, pieces, sems):
+            self.ref, self.pieces = ref, pieces
+            self.lanes = {
+                lane: (sems[2 * j], sems[2 * j + 1])
+                for j, lane in enumerate(("up", "down", "across", "side"))
+            }
+            self.turned = tuple(range(pieces // 2, pieces)) if paired else ()
 
         def copy(self, lane, block, piece, slot, target):
             sends, recvs = self.lanes[lane]
-            ref = self.view(block, piece)
+            ref = self.ref.at[block * self.pieces + piece]
             return pltpu.make_async_remote_copy(
                 src_ref=ref,
                 dst_ref=ref,
@@ -516,208 +546,310 @@
             return self.copy(lane, block_of(at, y), piece, slot, target)
 
         def sends(self, k, piece, act):
-            for lane, at, has, onward, slot in (
-                ("up", z - k, z >= k, z + 1 < line, max(2 * k - 1, 0)),
-                ("down", z + k, z + k < line, z > 0, 2 * k),
+            for lane, at, has, onward, slot, odd in (
+                ("up", z - k, z >= k, z + 1 < line, max(2 * k - 1, 0), 0),
+                ("down", z + k, z + k < line, z > 0, 2 * k, 1),
             ):
                 if k < line - 1:
                     pl.when(has & onward)(lambda: act(self.hop(lane, at, piece, k)))
                 if inner > 1 and (k > 0 or lane == "up"):
+                    if k == 1 and piece in self.turned:
+                        has = has & (lax.rem(z, 2) == odd)
                     pl.when(has)(lambda: act(self.hop("across", at, piece, slot)))
 
-        def start(self):
+        def start(self, piece):
+            self.sends(0, piece, lambda c: c.start())
+
+        def step(self, k, piece):
+            for lane, at, has in (("up", z - k, z >= k), ("down", z + k, z + k < line)):
+                pl.when(has)(lambda: self.hop(lane, at, piece, k - 1).wait_recv())
+            self.sends(k, piece, lambda c: c.start())
+
+        def side(self, piece):
+            return self.copy(
+                "side", block_of(z, inner - 1 - y), piece, 0, block_of(mate, y)
+            )
+
+        def side_start(self, when, piece):
+            pl.when(when)(lambda: self.side(piece).start())
+
+        def arrive(self, i, piece):
+            at = level(i)
+            block = block_of(at, inner - 1 - y)
+            slot = jnp.where(at < z, 2 * (z - at) - 1, 2 * (at - z))
+
+            def plain():
+                self.copy("across", block, piece, slot, block).wait_recv()
+
+            if i == 0 or piece not in self.turned:
+                plain()
+                return
+            pl.when(at != mate)(plain)
+            pl.when(at == mate)(
+                lambda: self.copy("side", block, piece, 0, block).wait_recv()
+            )
+
+        def drain(self):
             for piece in range(self.pieces):
-                self.sends(0, piece, lambda c: c.start())
-
-        def step(self, k):
-            for piece in range(self.pieces):
-                for lane, at, has in (("up", z - k, z >= k), ("down", z + k, z + k < line)):
-                    pl.when(has)(lambda: self.hop(lane, at, piece, k - 1).wait_recv())
-                self.sends(k, piece, lambda c: c.start())
-
-        def column(self, k, work):
-            pl.when(z >= k)(lambda: work(block_of(z - k, y)))
-            pl.when(z + k < line)(lambda: work(block_of(z + k, y)))
-
-        def other(self, k, work):
-            if inner == 1:
-                return
-
-            def arrive(at, slot):
-                block = block_of(at, inner - 1 - y)
-                for piece in range(self.pieces):
-                    self.copy("across", block, piece, slot, block).wait_recv()
-                work(block)
-
-            if k == 0:
-                arrive(z, 0)
-                return
-            pl.when(z >= k)(lambda: arrive(z - k, 2 * k - 1))
-            pl.when(z + k < line)(lambda: arrive(z + k, 2 * k))
-
-        def drain(self):
-            for k in range(line):
-                for piece in range(self.pieces):
+                for k in range(line):
                     self.sends(k, piece, lambda c: c.wait_send())
-
-    both = rows + crows
-    cut = both // 32 * 16
-
-    def x_view(block, piece):
-        part = pl.ds(0, cut) if piece == 0 else pl.ds(cut, both - cut)
-        return x_all.at[part, pl.ds(pl.multiple_of(block * feats, feats), feats)]
-
-    xg = Gather(x_view, 2, (xs_up, xr_up), (xs_dn, xr_dn), (xs_y, xr_y))
-    for copy in own_x:
+                if piece in self.turned:
+                    self.side(piece).wait_send()
+
+    def run(events):
+        for _, act in sorted(enumerate(events), key=lambda e: (e[1][0], e[0])):
+            act[1]()
+
+    xg = Gather(x_all, parts, gather_sems[:8])
+    hg = Gather(ho_all, hparts, gather_sems[8:16])
+
+    for copy in own_x[0]:
         copy.wait()
-    xg.start()
+    xg.start(0)
+    for pair in own_x[1:]:
+        for copy in pair:
+            copy.wait()
+
+    ones = jnp.ones((16, width), jnp.bfloat16)
+    row_sum = jnp.zeros((16, both), f32)
+    row_squares = jnp.zeros((16, both), f32)
+    for p in range(parts):
+        own = x_all[me * parts + p]
+        own_f = own.astype(f32)
+        row_sum = row_sum + nt(ones, own)
+        for part in terms(own_f * own_f):
+            row_squares = row_squares + nt(ones, part)
+    stat_all[me] = jnp.zeros(stat_all.shape[1:], f32)
+    stat_all[me, 0:1, 0:both] = row_sum[0:1]
+    stat_all[me, 1:2, 0:both] = row_squares[0:1]
+    sa = [
+        send(stat_all.at[me], stat_all.at[me], sa_s.at[d - 1], sa_r.at[d - 1], "tp", d)
+        for d in range(1, n)
+    ]
+    for p in range(1, parts):
+        xg.start(p)
 
     for copy in first:
         copy.wait()
+
     def one_row(which):
-        part = cond_v[which].astype(jnp.float32)
+        part = cond_v[which].astype(f32)
         return jnp.concatenate([part[r : r + 1] for r in range(part.shape[0])], axis=1)
 
     row_of = lax.broadcasted_iota(jnp.int32, (16, shift_m.shape[1]), 0)
     conds = jnp.where(row_of == 0, one_row(0), one_row(1))
     conds = short(conds * lax.logistic(conds))
-    for which in range(3):
+    for which in range(2):
         mod_own[2 * which : 2 * which + 2, :] = nt(conds, mod_w[which])[0:2]
-    mod_own[6:8, :] = jnp.zeros((2, feats), jnp.float32)
-    m1 = {
-        d: send(mod_own, mod_recv.at[d - 1], m1_s, m1_r, "sp", d) for d in range(1, s)
-    }
-
-    own = x_all[:, mine]
-    ones = jnp.ones((16, feats), jnp.bfloat16)
-    own_f = own.astype(jnp.float32)
-    rest = own_f * own_f
-    row_squares = jnp.zeros((16, both), jnp.float32)
-    for _ in range(3):
-        top = short(rest)
-        row_squares = row_squares + nt(ones, top)
-        rest = rest - top.astype(jnp.float32)
-    row_sum = nt(ones, own)
-
-    if line > 1:
-        xg.step(1)
-    for d in range(1, s):
-        m1[d].wait_recv()
-    total = mod_own[...]
-    for d in range(1, s):
-        total = total + mod_recv[d - 1]
-    mod_all[:, mine] = total
-    stat_cols = pl.ds(pl.multiple_of(me * feats, feats), both)
-    mod_all[6:7, stat_cols] = row_sum[0:1]
-    mod_all[7:8, stat_cols] = row_squares[0:1]
-    m2 = {
-        d: send(mod_all.at[:, mine], mod_all.at[:, mine], m2_s, m2_r, "tp", d)
-        for d in range(1, n)
-    }
+    m1 = [
+        send(mod_own, mod_recv.at[d - 1], m1_s.at[d - 1], m1_r.at[d - 1], "sp", d)
+        for d in range(1, s)
+    ]
+
+    def exchange_mods():
+        for copy in m1:
+            copy.wait_recv()
+        total = mod_own[...]
+        for d in range(1, s):
+            total = total + mod_recv[d - 1]
+        mod_all[me] = total
+        return [
+            send(mod_all.at[me], mod_all.at[me], m2_s.at[d - 1], m2_r.at[d - 1], "tp", d)
+            for d in range(1, n)
+        ]
+
+    held = {}
+
+    def send_mods():
+        held["m2"] = exchange_mods()
+
+    def send_gates():
+        gate_load.wait()
+        gate_own[...] = nt(conds, mod_w[2])[0:2]
+        held["mg"] = [
+            send(gate_own, gate_recv.at[d - 1], mg_s.at[d - 1], mg_r.at[d - 1], "sp", d)
+            for d in range(1, s)
+        ]
+
+    def early():
+        for copy in small:
+            copy.wait()
+        slot_head = lax.broadcasted_iota(jnp.int32, (spike_v.shape[1], hk), 0)
+        lane_head = lax.broadcasted_iota(jnp.int32, (spike_v.shape[1], hk), 1) // DK
+        pick = jnp.where(slot_head == me * heads + lane_head, 1.0, 0.0).astype(jnp.bfloat16)
+        for e in range(2):
+            spike_rows[:, e * hk : (e + 1) * hk] = sum(
+                tn(part, pick) for part in terms(spike_v[e])
+            )
+        acc[...] = jnp.zeros(acc.shape, f32)
+        low_acc[...] = jnp.zeros(low_acc.shape, f32)
+
+    def moments():
+        for copy in sa:
+            copy.wait_recv()
+        stats = sum(stat_all[b] for b in range(n))
+        diagonal = lax.broadcasted_iota(jnp.int32, (both, both), 0) == lax.broadcasted_iota(
+            jnp.int32, (both, both), 1
+        )
+
+        def column_of(row):
+            return (
+                jnp.sum(
+                    jnp.where(diagonal, stats[row : row + 1, 0:both], 0.0), axis=1, keepdims=True
+                )
+                / model
+            )
+
+        mean = column_of(0)
+        held["mean"] = mean
+        held["spread"] = lax.rsqrt(column_of(1) - mean * mean + epsilon)
+
+    def wait_mods():
+        for copy in held["m2"]:
+            copy.wait_recv()
+        for copy in weights:
+            copy.wait()
+
     tile = math.gcd(2 * hk + 2 * hv, 512)
     columns = acc.shape[1]
-    acc[...] = jnp.zeros(acc.shape, jnp.float32)
-    low_acc[...] = jnp.zeros(low_acc.shape, jnp.float32)
-
-    def moments():
-        for d in range(1, n):
-            m2[d].wait_recv()
-        diagonal = lax.broadcasted_iota(jnp.int32, (both, both), 0) == lax.broadcasted_iota(
-            jnp.int32, (both, both), 1
-        )
-
-        def column_of(row):
-            whole_row = sum(mod_all[row : row + 1, b * feats : b * feats + both] for b in range(n))
-            return jnp.sum(jnp.where(diagonal, whole_row, 0.0), axis=1, keepdims=True) / model
-
-        mean = column_of(6)
-        return mean, lax.rsqrt(column_of(7) - mean * mean + epsilon)
-
-    def project_block(block, mean, spread):
+
+    def project_block(block):
         cols = pl.ds(pl.multiple_of(block * feats, feats), feats)
-        x = (x_all[:, cols].astype(jnp.float32) - mean) * spread
-        mod = mod_all[:, cols]
-        xn[0:rows, :] = short(x[0:rows] * (1.0 + mod[2:3]) + mod[0:1])
-        xn[rows:, :] = short(x[rows:] * (1.0 + mod[3:4]) + mod[1:2])
+        mean, spread = held["mean"], held["spread"]
+        mod = mod_all[block]
+        for p in range(parts):
+            lanes = slice(p * width, (p + 1) * width)
+            x = (x_all[block * parts + p].astype(f32) - mean) * spread
+            m = mod[:, lanes]
+            xn[0:rows, lanes] = short(x[0:rows] * (1.0 + m[2:3]) + m[0:1])
+            xn[rows:, lanes] = short(x[rows:] * (1.0 + m[3:4]) + m[1:2])
         low_acc[...] += nt(xn[...], down_v[:, cols])
-
         for t in range(columns // tile):
             out = slice(t * tile, (t + 1) * tile)
             acc[:, out] += nt(xn[...], proj_w[out, cols])
 
-    ready = None
-    for k in range(2, line + 1):
-        if k < line:
-            xg.step(k)
-        if ready is None:
-            ready = moments()
-            for copy in weights:
-                copy.wait()
-            work = lambda block: project_block(block, *ready)
-            work(me)
-        xg.column(k - 1, work)
-        xg.other(k - 2, work)
-    xg.other(line - 1, work)
+    def column_block(i):
+        project_block(block_of(level(i), y))
+
+    def other_block(i):
+        if i > 0:
+            for p in range(parts):
+                xg.arrive(i, p)
+        project_block(block_of(level(i), inner - 1 - y))
+
+    unit, lag, cost = 0.79, 1.8, 0.68
+    arrival = lambda k, p: unit * ((k - 1) * parts + p + 1) + lag
+    events = [
+        (arrival(1, parts // 2 - 1) + 0.01, send_mods),
+        (arrival(1, parts // 2 - 1) + 0.02, send_gates),
+        (arrival(1, parts - 1) + 0.05, early),
+        (arrival(1, parts - 1) + 0.06, moments),
+        (arrival(2, parts // 2) + 0.01, wait_mods),
+    ]
+    for k in range(1, line):
+        for p in range(parts):
+            events.append((arrival(k, p), functools.partial(xg.step, k, p)))
+    if inner > 1:
+        for p in range(parts):
+            events.append((arrival(1, p) + 0.03, functools.partial(xg.arrive, 0, p)))
+            if p in xg.turned:
+                events.append(
+                    (arrival(1, p) + 0.04, functools.partial(xg.side_start, at_end, p))
+                )
+                if line > 2:
+                    events.append(
+                        (
+                            arrival(line - 2, parts - 1) + 0.01,
+                            functools.partial(
+                                xg.side_start, jnp.logical_not(at_end), p
+                            ),
+                        )
+                    )
+    tasks = []
+    for i in range(line):
+        ready = arrival(i, parts - 1) + 0.02 if i else 0.0
+        tasks.append((ready, functools.partial(column_block, i)))
+        if inner > 1:
+            ready = arrival(max(i, 1), parts - 1) + 0.05 + (lag if i else 0)
+            if i == 1 and xg.turned:
+                ready = max(ready, arrival(line - 1, parts - 1) + unit * len(xg.turned))
+            tasks.append((ready, functools.partial(other_block, i)))
+    clock = arrival(2, parts // 2) + 0.02
+    for ready, task in sorted(tasks, key=lambda t: t[0]):
+        clock = max(clock, ready)
+        events.append((clock, task))
+        clock += cost
+    run(events)
     proj[...] = short(acc[...])
 
     own_ctx = pl.ds(pl.multiple_of(sp * crows, crows), crows)
     ctx_kv[own_ctx, :] = proj[rows:, hk : 2 * hk + hv]
-    ctx_low[own_ctx, :] = jnp.zeros((crows, ctx_low.shape[1]), jnp.float32)
+    ctx_low[own_ctx, :] = jnp.zeros((crows, ctx_low.shape[1]), f32)
     ctx_low[own_ctx, 0 : 2 * DECAY_RANK] = low_acc[rows:]
-    kv = {
-        d: send(ctx_kv.at[own_ctx], ctx_kv.at[own_ctx], kv_s, kv_r, "sp", d)
+    kv = [
+        send(ctx_kv.at[own_ctx], ctx_kv.at[own_ctx], kv_s.at[d - 1], kv_r.at[d - 1], "sp", d)
         for d in range(1, s)
-    }
-    lo = {
-        d: send(ctx_low.at[own_ctx], ctx_low.at[own_ctx], lo_s, lo_r, "sp", d)
+    ]
+    lo = [
+        send(ctx_low.at[own_ctx], ctx_low.at[own_ctx], lo_s.at[d - 1], lo_r.at[d - 1], "sp", d)
         for d in range(1, s)
-    }
-
-    for copy in small:
-        copy.wait()
-    slot_head = lax.broadcasted_iota(jnp.int32, (spike_v.shape[1], hk), 0)
-    lane_head = lax.broadcasted_iota(jnp.int32, (spike_v.shape[1], hk), 1) // DK
-    pick = jnp.where(slot_head == me * heads + lane_head, 1.0, 0.0)
-    none = jnp.zeros((DECAY_RANK, hk), jnp.float32)
-    ups = [
-        jnp.concatenate([up_v[0].astype(jnp.float32), none], axis=0),
-        jnp.concatenate([none, up_v[1].astype(jnp.float32)], axis=0),
     ]
-    cum = []
-    for direction in range(2):
-        logs = log_decay_of(low_acc[0:rows], ups[direction], bias_v[direction : direction + 1])
-        logs = logs + lax.dot_general(
-            spike_v[direction],
-            pick,
-            (((0,), (0,)), ((), ())),
-            precision=precise,
-            preferred_element_type=jnp.float32,
-        )
-        cum.append(exact(triangle_of(rows, direction == 1).astype(jnp.float32), logs))
+
+    none = jnp.zeros((DECAY_RANK, hk), jnp.bfloat16)
+    up_both = jnp.concatenate(
+        [
+            jnp.concatenate([up_v[0], none], axis=1),
+            jnp.concatenate([none, up_v[1]], axis=1),
+        ],
+        axis=0,
+    )
+    bias_both = jnp.concatenate([bias_v[0:1], bias_v[1:2]], axis=1)
+
+    def logs_of(low):
+        return log_sigmoid(sum(nn(part, up_both) for part in terms(low)) + bias_both)
+
+    def running(logs, length, e):
+        lanes = slice(e * hk, (e + 1) * hk)
+        mask = jnp.where(triangle_of(length, e == 1), 1.0, 0.0).astype(jnp.bfloat16)
+        return sum(nn(mask, part) for part in terms(logs[:, lanes]))
+
+    logs = logs_of(low_acc[0:rows]) + spike_rows[...]
+    cum = [running(logs, rows, e) for e in range(2)]
     whole = [cum[0][rows - 1 : rows], cum[1][0:1]]
     tot_own[0:1, :] = whole[0]
     tot_own[1:2, :] = whole[1]
-    tot_own[2:8, :] = jnp.zeros((6, hk), jnp.float32)
-    to = {d: send(tot_own, tot_recv.at[d - 1], to_s, to_r, "sp", d) for d in range(1, s)}
-
-    keys = proj[0:rows, hk : 2 * hk].astype(jnp.float32)
-    for direction in range(2):
-        weighted = short(keys * jnp.exp(whole[direction] - cum[direction]))
-        for h in range(heads):
-            st_own[direction, h * DK : (h + 1) * DK, :] = short(
+    to = [
+        send(tot_own, tot_recv.at[d - 1], to_s.at[d - 1], to_r.at[d - 1], "sp", d)
+        for d in range(1, s)
+    ]
+
+    keys = proj[0:rows, hk : 2 * hk].astype(f32)
+    per = hparts // heads
+    weighted = [short(keys * jnp.exp(whole[e] - cum[e])) for e in range(2)]
+    st = {}
+    for h in range(heads):
+        for e in range(2):
+            state = short(
                 tn(
-                    weighted[:, h * DK : (h + 1) * DK],
+                    weighted[e][:, h * DK : (h + 1) * DK],
                     proj[0:rows, 2 * hk + h * dv : 2 * hk + (h + 1) * dv],
                 )
             )
-    st = {}
-    for d in range(1, s):
-        later = lax.rem(sp + d, s) > sp
-        st[d] = send(
-            st_own.at[jnp.where(later, 0, 1)], st_recv.at[d - 1], st_s, st_r, "sp", d
-        )
-
-    queries = proj[0:rows, 0:hk].astype(jnp.float32) * DK ** (-0.5)
+            for q in range(per):
+                st_own[e, h * per + q] = state[:, q * hwidth : (q + 1) * hwidth]
+        for q in range(h * per, (h + 1) * per):
+            for d in range(1, s):
+                later = lax.rem(sp + d, s) > sp
+                st[q, d] = send(
+                    st_own.at[jnp.where(later, 0, 1), q],
+                    st_recv.at[d - 1, q],
+                    st_s.at[d - 1, q],
+                    st_r.at[d - 1, q],
+                    "sp",
+                    d,
+                )
+
+    queries = proj[0:rows, 0:hk].astype(f32) * DK ** (-0.5)
     blocks = rows // BLK
 
     def span(b):
@@ -739,6 +871,7 @@
         for e in range(2)
     ]
     lower, upper = triangle_of(BLK, False), triangle_of(BLK, True)
+    scores = []
     for h in range(heads):
         ch = slice(h * DK, (h + 1) * DK)
         lines = []
@@ -759,59 +892,23 @@
                     near = short(queries[span(b)][:, ch] * jnp.exp(inside[e][b][:, ch] + gap))
                 strip.append(nt(near, k_end[e][c][:, ch]))
             lines.append(jnp.concatenate(strip, axis=1) if blocks > 1 else strip[0])
-        scores = short(jnp.concatenate(lines, axis=0) if blocks > 1 else lines[0])
-        local_out[:, h * dv : (h + 1) * dv] = nn(
-            scores, proj[0:rows, 2 * hk + h * dv : 2 * hk + (h + 1) * dv]
-        )
-
-    for d in range(1, s):
-        kv[d].wait_recv()
-        lo[d].wait_recv()
-    ctx_keys = ctx_kv[:, 0:hk].astype(jnp.float32)
-    ctx_states = []
-    for direction in range(2):
-        logs = log_decay_of(
-            ctx_low[:, 0 : 2 * DECAY_RANK],
-            ups[direction],
-            bias_v[direction : direction + 1],
-        )
-        length = s * crows
-        c = exact(triangle_of(length, direction == 1).astype(jnp.float32), logs)
-        end = c[length - 1 : length] if direction == 0 else c[0:1]
-        weighted = short(ctx_keys * jnp.exp(end - c))
-        ctx_states.append(
-            [
-                short(
-                    tn(
-                        weighted[:, h * DK : (h + 1) * DK],
-                        ctx_kv[:, hk + h * dv : hk + (h + 1) * dv],
-                    )
-                )
-                for h in range(heads)
-            ]
-        )
-
-    for d in range(1, s):
-        to[d].wait_recv()
+        scores.append(short(jnp.concatenate(lines, axis=0) if blocks > 1 else lines[0]))
+
+    for copy in to:
+        copy.wait_recv()
     places = {d: lax.rem(sp - d + s, s) for d in range(1, s)}
 
     def passed(low_end, high_end, direction):
-        result = jnp.zeros((1, hk), jnp.float32)
+        result = jnp.zeros((1, hk), f32)
         for d in range(1, s):
-            held = jnp.where((places[d] > low_end) & (places[d] < high_end), 1.0, 0.0)
-            result = result + held * tot_recv[d - 1][direction : direction + 1]
+            inside_it = jnp.where((places[d] > low_end) & (places[d] < high_end), 1.0, 0.0)
+            result = result + inside_it * tot_recv[d - 1][direction : direction + 1]
         return result
 
     ctx_reach = [
         short(queries * jnp.exp(cum[0] + passed(-1, sp, 0))),
         short(queries * jnp.exp(cum[1] + passed(sp, s, 1))),
     ]
-    for h in range(heads):
-        ch = slice(h * DK, (h + 1) * DK)
-        local_out[:, h * dv : (h + 1) * dv] += nn(
-            jnp.concatenate([r[:, ch] for r in ctx_reach], axis=1),
-            jnp.concatenate([ctx_states[e][h] for e in range(2)], axis=0),
-        )
     reach = []
     for d in range(1, s):
         p = places[d]
@@ -820,44 +917,114 @@
             cum[1] + passed(sp, p, 1)
         )
         reach.append(short(queries * jnp.exp(exponent)))
-    gate_rows = proj[0:rows, 2 * hk + hv :].astype(jnp.float32)
+    gate_rows = proj[0:rows, 2 * hk + hv :].astype(f32)
     small_gate = gate_rows * lax.logistic(gate_rows) * gain_v[...]
-    gi = lax.broadcasted_iota(jnp.int32, (dv, dv), 0) // VGROUP
-    gj = lax.broadcasted_iota(jnp.int32, (dv, dv), 1) // VGROUP
-    group = jnp.where(gi == gj, 1.0, 0.0).astype(jnp.bfloat16)
-    for d in range(1, s):
-        st[d].wait_recv()
+
+    for copy in kv + lo:
+        copy.wait_recv()
+    ctx_keys = ctx_kv[:, 0:hk].astype(f32)
+    ctx_logs = logs_of(ctx_low[:, 0 : 2 * DECAY_RANK])
+    length = s * crows
+    ctx_weighted = []
+    for e in range(2):
+        c = running(ctx_logs, length, e)
+        end = c[length - 1 : length] if e == 0 else c[0:1]
+        ctx_weighted.append(short(ctx_keys * jnp.exp(end - c)))
     for h in range(heads):
         ch = slice(h * DK, (h + 1) * DK)
         vc = slice(h * dv, (h + 1) * dv)
-        o = local_out[:, vc]
+        ctx_values = ctx_kv[:, hk + h * dv : hk + (h + 1) * dv]
+        local_out[:, vc] = nn(
+            jnp.concatenate([scores[h]] + [r[:, ch] for r in ctx_reach], axis=1),
+            jnp.concatenate(
+                [proj[0:rows, 2 * hk + h * dv : 2 * hk + (h + 1) * dv]]
+                + [short(tn(w[:, ch], ctx_values)) for w in ctx_weighted],
+                axis=0,
+            ),
+        )
+    gi = lax.broadcasted_iota(jnp.int32, (hwidth, hwidth), 0) // VGROUP
+    gj = lax.broadcasted_iota(jnp.int32, (hwidth, hwidth), 1) // VGROUP
+    group = jnp.where(gi == gj, 1.0, 0.0).astype(jnp.bfloat16)
+
+    def head_piece(q):
+        h = q // per
+        ch = slice(h * DK, (h + 1) * DK)
+        vc = slice(q * hwidth, (q + 1) * hwidth)
         for d in range(1, s):
-            o = o + nn(reach[d - 1][:, ch], st_recv[d - 1, ch, :])
+            st[q, d].wait_recv()
+        o = local_out[:, vc] + nn(
+            jnp.concatenate([r[:, ch] for r in reach], axis=1),
+            jnp.concatenate([st_recv[d - 1, q] for d in range(1, s)], axis=0),
+        )
         squares = o * o
         top = short(squares)
-        rest = short(squares - top.astype(jnp.float32))
+        rest = short(squares - top.astype(f32))
         power = (nn(top, group) + nn(rest, group)) * (1.0 / VGROUP)
-        ho_all[me, :, vc] = short(o * lax.rsqrt(power + epsilon) * small_gate[:, vc])
-
-    def ho_view(block, piece):
-        return ho_all.at[block, pl.ds(piece * (rows // 4), rows // 4)]
-
-    hg = Gather(ho_view, 4, (hs_up, hr_up), (hs_dn, hr_dn), (hs_y, hr_y))
-    hg.start()
-    last.wait()
-    local_out[...] = nt(ho_all[me], out_w[:, mine])
-
-    def add_block(block):
-        cols = pl.ds(pl.multiple_of(block * feats, feats), feats)
-        local_out[...] += nt(ho_all[block], out_w[:, cols])
-
-    for k in range(1, line):
-        hg.step(k)
-        hg.other(k - 1, add_block)
-        hg.column(k, add_block)
-    hg.other(line - 1, add_block)
-    gates = mod_all[:, mine][4:5]
-    out_ref[...] = short(x_all[0:rows, mine].astype(jnp.float32) + gates * local_out[...])
+        ho_all[me * hparts + q] = short(o * lax.rsqrt(power + epsilon) * small_gate[:, vc])
+        hg.start(q)
+
+    def ready_out():
+        last.wait()
+        for copy in held["mg"]:
+            copy.wait_recv()
+        total_out[...] = jnp.zeros(total_out.shape, f32)
+
+    def add_half(block, half):
+        cols = pl.ds(pl.multiple_of(block * feats + half * 2 * hwidth, 2 * hwidth), 2 * hwidth)
+        pair = jnp.concatenate(
+            [ho_all[block * hparts + 2 * half], ho_all[block * hparts + 2 * half + 1]], axis=1
+        )
+        total_out[...] += nt(pair, out_w[:, cols])
+
+    def add_column(i, half):
+        add_half(block_of(level(i), y), half)
+
+    def add_other(i, half):
+        if i > 0:
+            hg.arrive(i, 2 * half)
+            hg.arrive(i, 2 * half + 1)
+        add_half(block_of(level(i), inner - 1 - y), half)
+
+    gap_h, hop_h = 1.4, 2.5
+    here = lambda k, q: gap_h * q + hop_h * k
+    events = [(here(0, 1) + 0.01, ready_out)]
+    for q in range(hparts):
+        events.append((here(0, q), functools.partial(head_piece, q)))
+        for k in range(1, line):
+            events.append((here(k, q), functools.partial(hg.step, k, q)))
+        if inner > 1:
+            events.append((here(1, q) + 0.02, functools.partial(hg.arrive, 0, q)))
+            if q in hg.turned:
+                events.append(
+                    (here(1, q) + 0.03, functools.partial(hg.side_start, at_end, q))
+                )
+                if line > 2:
+                    events.append(
+                        (
+                            here(line - 2, q) + 0.03,
+                            functools.partial(
+                                hg.side_start, jnp.logical_not(at_end), q
+                            ),
+                        )
+                    )
+    for i in range(line):
+        for half in range(hparts // 2):
+            when = here(i, 2 * half + 1) + 0.1
+            events.append((when, functools.partial(add_column, i, half)))
+            if inner > 1:
+                when += hop_h + 0.1
+                if i == 1 and 2 * half in hg.turned:
+                    when = max(when, here(line - 1, 2 * half + 1) + 0.4)
+                events.append((when, functools.partial(add_other, i, half)))
+    run(events)
+    gates = gate_own[0:1]
+    for d in range(1, s):
+        gates = gates + gate_recv[d - 1, 0:1]
+    for p in range(parts):
+        lanes = slice(p * width, (p + 1) * width)
+        out_ref[:, lanes] = short(
+            x_all[me * parts + p, 0:rows].astype(f32) + gates[:, lanes] * total_out[:, lanes]
+        )
     for copy in started:
         copy.wait_send()
     xg.drain()
@@ -892,11 +1059,14 @@
     model = n * feats
     both = rows + crows
     inputs = conditioning.shape[0]
+    parts = feats // 128
+    hparts = hv // 128
+    stat_width = -(-both // 128) * 128
     bf, f32 = jnp.bfloat16, jnp.float32
     vmem, dma = pltpu.VMEM, pltpu.SemaphoreType.DMA
-    pair = lambda k: [dma((k,)), dma((k,))]
+    pair = lambda *k: [dma(k), dma(k)]
     scratch = [
-        vmem((both, model), bf),
+        vmem((n * parts, both, 128), bf),
         vmem((both, feats), bf),
         vmem((both, 2 * hk + 2 * hv), f32),
         vmem((both, 2 * DECAY_RANK), f32),
@@ -909,30 +1079,37 @@
         vmem((2, HEADS, rows), f32),
         vmem((1, hv), f32),
         vmem((2, inputs // 128, 128), bf),
-        vmem((8, feats), f32),
-        vmem((s - 1, 8, feats), f32),
-        vmem((8, model), f32),
+        vmem((4, feats), f32),
+        vmem((s - 1, 4, feats), f32),
+        vmem((n, 4, feats), f32),
+        vmem((2, feats), f32),
+        vmem((s - 1, 2, feats), f32),
+        vmem((n, 2, stat_width), f32),
+        vmem((rows, 2 * hk), f32),
         vmem((both, 2 * hk + 2 * hv), bf),
         vmem((s * crows, hk + hv), bf),
         vmem((s * crows, 128), f32),
-        vmem((8, hk), f32),
-        vmem((s - 1, 8, hk), f32),
-        vmem((2, hk, dv), bf),
-        vmem((s - 1, hk, dv), bf),
+        vmem((2, hk), f32),
+        vmem((s - 1, 2, hk), f32),
+        vmem((2, hparts, DK, 128), bf),
+        vmem((s - 1, hparts, DK, 128), bf),
         vmem((rows, hv), f32),
-        vmem((n, rows, hv), bf),
-        dma((17,)),
+        vmem((n * hparts, rows, 128), bf),
+        vmem((rows, feats), f32),
+        dma((15 + 2 * parts,)),
     ]
+    for counts in ((s - 1,), (n - 1,), (s - 1,), (n - 1,), (s - 1,), (s - 1,), (s - 1,), (s - 1, hparts)):
+        scratch += pair(*counts)
     inner = 2 if n % 2 == 0 else 1
     line = n // inner
     hops = max(line - 1, 1)
-    counts = (hops, hops, hops, hops, 2 * line - 1, 2 * line - 1)
-    scratch += [dma((k, 2)) for k in counts]
-    for count in (s - 1, n - 1, s - 1, s - 1, s - 1, s - 1):
-        scratch += pair(count)
-    scratch += [dma((k, 4)) for k in counts]
+    for pieces in (parts, hparts):
+        for count in (hops, hops, 2 * line - 1, 1):
+            scratch += pair(count, pieces)
     return pl.pallas_call(
-        functools.partial(layer_kernel, n, s, inner, rows, crows, feats, heads, dv),
+        functools.partial(
+            layer_kernel, n, s, inner, rows, crows, feats, heads, dv, parts, hparts
+        ),
         out_shape=jax.ShapeDtypeStruct((rows, feats), bf),
         in_specs=[pl.BlockSpec(memory_space=pl.ANY)] * 17,
         out_specs=pl.BlockSpec(memory_space=pltpu.VMEM),

time: 50.8 us -> 52.5 us (1.033)
  Pallas kernels: 49 us -> 50.8 us
    pallas_call x1, Pallas kernels: 49 us -> 50.8 us  [one_kernel(): pl.pallas_call(functools.partial(layer_kernel, n, s, inner, rows, crows,...]
where the time goes in v1:
time: 52.5 us; the launch traced here: 52.4 us
  Pallas kernels  50.8 us (97%)
  local copies, waits for them, and re-layouts  1.57 us (3%)
    pallas_call x1, Pallas kernels, one_kernel(): pl.pallas_call(functools.partial(layer_kernel, n, s, inner, rows, crows,...  50.8 us
    unnamed x1, local copies, waits for them, and re-layouts  1.57 us

profile of v1, /device:TPU:0, one launch (start us, length us, event | category | flops | bytes accessed | tf_op | source)
XLA Modules:
  0.0 52.4 jit_solution(3906631306478992306)
XLA Ops:
  0.0 50.8 %layer.1 = bf16[128,512]{1,0:T(8,128)(2,1)} custom-call(bf16[128,512]{1,0:T(8,128)(2,1)} %latent.1, bf16[16,512]{1,0:T(8,128)(2,1)} %context.1, bf16[8,128]{1,0:T(8,128)(2,1)} %bitcast.9, bf16[8,128]{1,0:T(8,128)(2,1)} %bitcast.10, bf16[512,1024]{1,0:T(8,128)(2,1)} %shift_m.1, bf16[512,1024]{1,0:T(8,128)(2,1)} %scale_m.1, bf16[512,1024]{1,0:T(8,128)(2,1)} %gate_m.1, ...), custom_call_target="tpu_custom_call" | custom-call | tf_op jit(solution)/shard_map/layer/pallas_call | solution.py:1109
  50.8 1.6 %copy.19 = bf16[128,512]{1,0:T(8,128)(2,1)} copy(bf16[128,512]{1,0:T(8,128)(2,1)} %layer.1) | data formatting | bytes 262144

commit v2 on v1

--- a/solution.py
+++ b/solution.py
@@ -324,6 +324,10 @@
 
 def short(value):
     return value.astype(jnp.bfloat16)
+
+
+X_STRAIGHT = ()
+H_STRAIGHT = ()
 
 
 def terms(value):
@@ -517,8 +521,8 @@
         return at * inner + column
 
     class Gather:
-        def __init__(self, ref, pieces, sems):
-            self.ref, self.pieces = ref, pieces
+        def __init__(self, ref, pieces, straight, sems):
+            self.ref, self.pieces, self.straight = ref, pieces, straight
             self.lanes = {
                 lane: (sems[2 * j], sems[2 * j + 1])
                 for j, lane in enumerate(("up", "down", "across", "side"))
@@ -545,25 +549,48 @@
             }[lane]
             return self.copy(lane, block_of(at, y), piece, slot, target)
 
+        def reach(self, piece, act):
+            for k in range(line - 1, 0, -1):
+                for lane, has, to in (("up", z + k < line, z + k), ("down", z >= k, z - k)):
+                    pl.when(has)(
+                        lambda: act(
+                            self.copy(lane, block_of(z, y), piece, k - 1, block_of(to, y))
+                        )
+                    )
+
+        def lane_sends(self, lane, k, piece, act):
+            up = lane == "up"
+            at, has = (z - k, z >= k) if up else (z + k, z + k < line)
+            slot = max(2 * k - 1, 0) if up else 2 * k
+            if k < line - 1 and piece not in self.straight:
+                onward = z + 1 < line if up else z > 0
+                pl.when(has & onward)(lambda: act(self.hop(lane, at, piece, k)))
+            if inner > 1 and (k > 0 or up):
+                if k == 1 and piece in self.turned:
+                    has = has & (lax.rem(z, 2) == (0 if up else 1))
+                pl.when(has)(lambda: act(self.hop("across", at, piece, slot)))
+
         def sends(self, k, piece, act):
-            for lane, at, has, onward, slot, odd in (
-                ("up", z - k, z >= k, z + 1 < line, max(2 * k - 1, 0), 0),
-                ("down", z + k, z + k < line, z > 0, 2 * k, 1),
-            ):
-                if k < line - 1:
-                    pl.when(has & onward)(lambda: act(self.hop(lane, at, piece, k)))
-                if inner > 1 and (k > 0 or lane == "up"):
-                    if k == 1 and piece in self.turned:
-                        has = has & (lax.rem(z, 2) == odd)
-                    pl.when(has)(lambda: act(self.hop("across", at, piece, slot)))
+            if k == 0 and piece in self.straight:
+                self.reach(piece, act)
+            for lane in ("up", "down"):
+                self.lane_sends(lane, k, piece, act)
 
         def start(self, piece):
             self.sends(0, piece, lambda c: c.start())
 
-        def step(self, k, piece):
-            for lane, at, has in (("up", z - k, z >= k), ("down", z + k, z + k < line)):
-                pl.when(has)(lambda: self.hop(lane, at, piece, k - 1).wait_recv())
-            self.sends(k, piece, lambda c: c.start())
+        def take(self, lane, k, piece):
+            at, has = (z - k, z >= k) if lane == "up" else (z + k, z + k < line)
+            pl.when(has)(lambda: self.hop(lane, at, piece, k - 1).wait_recv())
+            self.lane_sends(lane, k, piece, lambda c: c.start())
+
+        def near(self, k, piece):
+            pl.when(z >= line // 2)(lambda: self.take("up", k, piece))
+            pl.when(z < line // 2)(lambda: self.take("down", k, piece))
+
+        def far(self, k, piece):
+            pl.when(z < line // 2)(lambda: self.take("up", k, piece))
+            pl.when(z >= line // 2)(lambda: self.take("down", k, piece))
 
         def side(self, piece):
             return self.copy(
@@ -600,8 +627,8 @@
         for _, act in sorted(enumerate(events), key=lambda e: (e[1][0], e[0])):
             act[1]()
 
-    xg = Gather(x_all, parts, gather_sems[:8])
-    hg = Gather(ho_all, hparts, gather_sems[8:16])
+    xg = Gather(x_all, parts, X_STRAIGHT, gather_sems[:8])
+    hg = Gather(ho_all, hparts, H_STRAIGHT, gather_sems[8:16])
 
     for copy in own_x[0]:
         copy.wait()
@@ -737,18 +764,21 @@
                 xg.arrive(i, p)
         project_block(block_of(level(i), inner - 1 - y))
 
-    unit, lag, cost = 0.79, 1.8, 0.68
+    unit, lag, cost = 0.79, 2.0, 0.6
     arrival = lambda k, p: unit * ((k - 1) * parts + p + 1) + lag
+    mods_at = 9.4
     events = [
         (arrival(1, parts // 2 - 1) + 0.01, send_mods),
         (arrival(1, parts // 2 - 1) + 0.02, send_gates),
         (arrival(1, parts - 1) + 0.05, early),
         (arrival(1, parts - 1) + 0.06, moments),
-        (arrival(2, parts // 2) + 0.01, wait_mods),
+        (mods_at, wait_mods),
     ]
     for k in range(1, line):
         for p in range(parts):
-            events.append((arrival(k, p), functools.partial(xg.step, k, p)))
+            events.append((arrival(k, p), functools.partial(xg.near, k, p)))
+            if 2 * k < line + line % 2:
+                events.append((arrival(k, p) + 0.005, functools.partial(xg.far, k, p)))
     if inner > 1:
         for p in range(parts):
             events.append((arrival(1, p) + 0.03, functools.partial(xg.arrive, 0, p)))
@@ -774,7 +804,7 @@
             if i == 1 and xg.turned:
                 ready = max(ready, arrival(line - 1, parts - 1) + unit * len(xg.turned))
             tasks.append((ready, functools.partial(other_block, i)))
-    clock = arrival(2, parts // 2) + 0.02
+    clock = mods_at + 0.01
     for ready, task in sorted(tasks, key=lambda t: t[0]):
         clock = max(clock, ready)
         events.append((clock, task))
@@ -784,14 +814,15 @@
 
     own_ctx = pl.ds(pl.multiple_of(sp * crows, crows), crows)
     ctx_kv[own_ctx, :] = proj[rows:, hk : 2 * hk + hv]
-    ctx_low[own_ctx, :] = jnp.zeros((crows, ctx_low.shape[1]), f32)
-    ctx_low[own_ctx, 0 : 2 * DECAY_RANK] = low_acc[rows:]
+    ctx_low[own_ctx, :] = jnp.zeros((crows, ctx_low.shape[1]), jnp.bfloat16)
+    for i, part in enumerate(terms(low_acc[rows:])):
+        ctx_low[own_ctx, i * 2 * DECAY_RANK : (i + 1) * 2 * DECAY_RANK] = part
+    lo = [
+        send(ctx_low.at[own_ctx], ctx_low.at[own_ctx], lo_s.at[d - 1], lo_r.at[d - 1], "sp", d)
+        for d in range(1, s)
+    ]
     kv = [
         send(ctx_kv.at[own_ctx], ctx_kv.at[own_ctx], kv_s.at[d - 1], kv_r.at[d - 1], "sp", d)
-        for d in range(1, s)
-    ]
-    lo = [
-        send(ctx_low.at[own_ctx], ctx_low.at[own_ctx], lo_s.at[d - 1], lo_r.at[d - 1], "sp", d)
         for d in range(1, s)
     ]
 
@@ -805,15 +836,15 @@
     )
     bias_both = jnp.concatenate([bias_v[0:1], bias_v[1:2]], axis=1)
 
-    def logs_of(low):
-        return log_sigmoid(sum(nn(part, up_both) for part in terms(low)) + bias_both)
+    def logs_of(parts_of_low):
+        return log_sigmoid(sum(nn(part, up_both) for part in parts_of_low) + bias_both)
 
     def running(logs, length, e):
         lanes = slice(e * hk, (e + 1) * hk)
         mask = jnp.where(triangle_of(length, e == 1), 1.0, 0.0).astype(jnp.bfloat16)
         return sum(nn(mask, part) for part in terms(logs[:, lanes]))
 
-    logs = logs_of(low_acc[0:rows]) + spike_rows[...]
+    logs = logs_of(terms(low_acc[0:rows])) + spike_rows[...]
     cum = [running(logs, rows, e) for e in range(2)]
     whole = [cum[0][rows - 1 : rows], cum[1][0:1]]
     tot_own[0:1, :] = whole[0]
@@ -894,6 +925,19 @@
             lines.append(jnp.concatenate(strip, axis=1) if blocks > 1 else strip[0])
         scores.append(short(jnp.concatenate(lines, axis=0) if blocks > 1 else lines[0]))
 
+    for copy in lo:
+        copy.wait_recv()
+    low_parts = [
+        ctx_low[:, i * 2 * DECAY_RANK : (i + 1) * 2 * DECAY_RANK] for i in range(3)
+    ]
+    ctx_logs = logs_of(low_parts)
+    length = s * crows
+    ctx_decay = []
+    for e in range(2):
+        c = running(ctx_logs, length, e)
+        end = c[length - 1 : length] if e == 0 else c[0:1]
+        ctx_decay.append(jnp.exp(end - c))
+
     for copy in to:
         copy.wait_recv()
     places = {d: lax.rem(sp - d + s, s) for d in range(1, s)}
@@ -920,16 +964,10 @@
     gate_rows = proj[0:rows, 2 * hk + hv :].astype(f32)
     small_gate = gate_rows * lax.logistic(gate_rows) * gain_v[...]
 
-    for copy in kv + lo:
+    for copy in kv:
         copy.wait_recv()
     ctx_keys = ctx_kv[:, 0:hk].astype(f32)
-    ctx_logs = logs_of(ctx_low[:, 0 : 2 * DECAY_RANK])
-    length = s * crows
-    ctx_weighted = []
-    for e in range(2):
-        c = running(ctx_logs, length, e)
-        end = c[length - 1 : length] if e == 0 else c[0:1]
-        ctx_weighted.append(short(ctx_keys * jnp.exp(end - c)))
+    ctx_weighted = [short(ctx_keys * part) for part in ctx_decay]
     for h in range(heads):
         ch = slice(h * DK, (h + 1) * DK)
         vc = slice(h * dv, (h + 1) * dv)
@@ -985,13 +1023,15 @@
             hg.arrive(i, 2 * half + 1)
         add_half(block_of(level(i), inner - 1 - y), half)
 
-    gap_h, hop_h = 1.4, 2.5
-    here = lambda k, q: gap_h * q + hop_h * k
+    hop_h = 2.6
+    here = lambda k, q: 0.4 * q + 0.4 * (q // 2) + hop_h * k
     events = [(here(0, 1) + 0.01, ready_out)]
     for q in range(hparts):
         events.append((here(0, q), functools.partial(head_piece, q)))
         for k in range(1, line):
-            events.append((here(k, q), functools.partial(hg.step, k, q)))
+            events.append((here(k, q), functools.partial(hg.near, k, q)))
+            if 2 * k < line + line % 2:
+                events.append((here(k, q) + 0.5, functools.partial(hg.far, k, q)))
         if inner > 1:
             events.append((here(1, q) + 0.02, functools.partial(hg.arrive, 0, q)))
             if q in hg.turned:
@@ -1009,7 +1049,7 @@
                     )
     for i in range(line):
         for half in range(hparts // 2):
-            when = here(i, 2 * half + 1) + 0.1
+            when = here(i, 2 * half + 1) + 0.6
             events.append((when, functools.partial(add_column, i, half)))
             if inner > 1:
                 when += hop_h + 0.1
@@ -1088,7 +1128,7 @@
         vmem((rows, 2 * hk), f32),
         vmem((both, 2 * hk + 2 * hv), bf),
         vmem((s * crows, hk + hv), bf),
-        vmem((s * crows, 128), f32),
+        vmem((s * crows, 128), bf),
         vmem((2, hk), f32),
         vmem((s - 1, 2, hk), f32),
         vmem((2, hparts, DK, 128), bf),

time: 52.5 us -> 48.1 us (0.916)
  Pallas kernels: 50.8 us -> 46.4 us
    pallas_call x1, Pallas kernels: 50.8 us -> 46.4 us  [one_kernel(): pl.pallas_call(functools.partial(layer_kernel, n, s, inner, rows, crows,...]
where the time goes in v2:
time: 48.1 us; the launch traced here: 47.9 us
  Pallas kernels  46.4 us (96%)
  local copies, waits for them, and re-layouts  1.57 us (3%)
    pallas_call x1, Pallas kernels, one_kernel(): pl.pallas_call(functools.partial(layer_kernel, n, s, inner, rows, crows,...  46.4 us
    unnamed x1, local copies, waits for them, and re-layouts  1.57 us

profile of v2, /device:TPU:0, one launch (start us, length us, event | category | flops | bytes accessed | tf_op | source)
XLA Modules:
  0.0 47.9 jit_solution(13567837070230927434)
XLA Ops:
  0.0 46.4 %layer.1 = bf16[128,512]{1,0:T(8,128)(2,1)} custom-call(bf16[128,512]{1,0:T(8,128)(2,1)} %latent.1, bf16[16,512]{1,0:T(8,128)(2,1)} %context.1, bf16[8,128]{1,0:T(8,128)(2,1)} %bitcast.9, bf16[8,128]{1,0:T(8,128)(2,1)} %bitcast.10, bf16[512,1024]{1,0:T(8,128)(2,1)} %shift_m.1, bf16[512,1024]{1,0:T(8,128)(2,1)} %scale_m.1, bf16[512,1024]{1,0:T(8,128)(2,1)} %gate_m.1, ...), custom_call_target="tpu_custom_call" | custom-call | tf_op jit(solution)/shard_map/layer/pallas_call | solution.py:1149
  46.4 1.6 %copy.19 = bf16[128,512]{1,0:T(8,128)(2,1)} copy(bf16[128,512]{1,0:T(8,128)(2,1)} %layer.1) | data formatting | bytes 262144

commit v3 on v2

--- a/solution.py
+++ b/solution.py
@@ -324,10 +324,6 @@
 
 def short(value):
     return value.astype(jnp.bfloat16)
-
-
-X_STRAIGHT = ()
-H_STRAIGHT = ()
 
 
 def terms(value):
@@ -407,22 +403,8 @@
     ho_all,
     total_out,
     load_sem,
-    m1_s,
-    m1_r,
-    m2_s,
-    m2_r,
-    mg_s,
-    mg_r,
-    sa_s,
-    sa_r,
-    kv_s,
-    kv_r,
-    lo_s,
-    lo_r,
-    to_s,
-    to_r,
-    st_s,
-    st_r,
+    x_send,
+    x_recv,
     *gather_sems,
 ):
     me = lax.axis_index("tp")
@@ -435,45 +417,53 @@
     hwidth = hv // hparts
     f32 = jnp.float32
 
-    loads = []
-
-    def load(src, dst):
-        copy = pltpu.make_async_copy(src, dst, load_sem.at[len(loads)])
-        loads.append(copy)
-        copy.start()
-        return copy
-
-    own_x = []
-    for p in range(parts):
+    used = [0]
+
+    def load(*pairs, whole):
+        sem = load_sem.at[used[0]]
+        used[0] += 1
+        for src, dst in pairs:
+            pltpu.make_async_copy(src, dst, sem).start()
+        return pltpu.make_async_copy(whole, whole, sem)
+
+    def own_piece(p):
         cols = pl.ds(p * width, width)
+        return (
+            (latent.at[:, cols], x_all.at[me * parts + p, pl.ds(0, rows)]),
+            (context.at[:, cols], x_all.at[me * parts + p, pl.ds(rows, crows)]),
+        )
+
+    own_x = [load(*own_piece(0), whole=x_all.at[pl.ds(me * parts, 1)])]
+    if parts > 1:
         own_x.append(
-            (
-                load(latent.at[:, cols], x_all.at[me * parts + p, pl.ds(0, rows)]),
-                load(context.at[:, cols], x_all.at[me * parts + p, pl.ds(rows, crows)]),
+            load(
+                *[c for p in range(1, parts) for c in own_piece(p)],
+                whole=x_all.at[pl.ds(me * parts + 1, parts - 1)],
             )
         )
     first = [
-        load(conditioning, cond_v.at[0]),
-        load(prompt, cond_v.at[1]),
-        load(shift_m, mod_w.at[0]),
-        load(scale_m, mod_w.at[1]),
+        load((conditioning, cond_v.at[0]), (prompt, cond_v.at[1]), whole=cond_v),
+        load((shift_m, mod_w.at[0]), (scale_m, mod_w.at[1]), whole=mod_w.at[pl.ds(0, 2)]),
     ]
-    gate_load = load(gate_m, mod_w.at[2])
+    gate_load = load((gate_m, mod_w.at[2]), whole=mod_w.at[2])
     head_cols = pl.ds(pl.multiple_of(me * hk, hk), hk)
     small = [
-        load(up.at[:, :, head_cols], up_v),
-        load(bias.at[:, head_cols], bias_v),
-        load(spike, spike_v),
-        load(gain, gain_v),
+        load((up.at[:, :, head_cols], up_v), whole=up_v),
+        load((bias.at[:, head_cols], bias_v), whole=bias_v),
+        load((spike, spike_v), whole=spike_v),
+        load((gain, gain_v), whole=gain_v),
     ]
     weights = [
-        load(query_m, proj_w.at[pl.ds(0, hk)]),
-        load(key_m, proj_w.at[pl.ds(hk, hk)]),
-        load(value_m, proj_w.at[pl.ds(2 * hk, hv)]),
-        load(og_m, proj_w.at[pl.ds(2 * hk + hv, hv)]),
-        load(down, down_v),
+        load(
+            (query_m, proj_w.at[pl.ds(0, hk)]),
+            (key_m, proj_w.at[pl.ds(hk, hk)]),
+            (value_m, proj_w.at[pl.ds(2 * hk, hv)]),
+            (og_m, proj_w.at[pl.ds(2 * hk + hv, hv)]),
+            whole=proj_w,
+        ),
+        load((down, down_v), whole=down_v),
     ]
-    last = load(out_m, out_w)
+    last = load((out_m, out_w), whole=out_w)
 
     barrier = pltpu.get_barrier_semaphore()
     for d in range(1, n):
@@ -488,19 +478,31 @@
 
     started = []
 
-    def send(src, dst, send_sem, recv_sem, axis, d):
-        index, count = (me, n) if axis == "tp" else (sp, s)
-        copy = pltpu.make_async_remote_copy(
-            src_ref=src,
-            dst_ref=dst,
-            send_sem=send_sem,
-            recv_sem=recv_sem,
-            device_id={axis: lax.rem(index + d, count)},
-            device_id_type=MESH,
-        )
-        copy.start()
-        started.append(copy)
-        return copy
+    class Exchange:
+        def __init__(self, axis, index, src, dst, landed, send_index=None, sent=True):
+            at, count = (me, n) if axis == "tp" else (sp, s)
+            self.some = count > 1
+
+            def copy(source, target, d):
+                return pltpu.make_async_remote_copy(
+                    src_ref=source,
+                    dst_ref=target,
+                    send_sem=x_send.at[index if send_index is None else send_index],
+                    recv_sem=x_recv.at[index],
+                    device_id={axis: lax.rem(at + d, count)},
+                    device_id_type=MESH,
+                )
+
+            for d in range(1, count):
+                copy(src(d), dst(d), d).start()
+            if self.some:
+                self.all = copy(landed, landed, 1)
+                if sent:
+                    started.append(self.all)
+
+        def wait_recv(self):
+            if self.some:
+                self.all.wait_recv()
 
     line = n // inner
     z, y = lax.div(me, inner), lax.rem(me, inner)
@@ -521,67 +523,58 @@
         return at * inner + column
 
     class Gather:
-        def __init__(self, ref, pieces, straight, sems):
-            self.ref, self.pieces, self.straight = ref, pieces, straight
-            self.lanes = {
-                lane: (sems[2 * j], sems[2 * j + 1])
-                for j, lane in enumerate(("up", "down", "across", "side"))
-            }
+        def __init__(self, ref, pieces, sems):
+            self.ref, self.pieces = ref, pieces
+            self.column_send, self.across_send, self.column_recv, self.across_recv = sems
+            self.half = max(pieces // 2, 1)
             self.turned = tuple(range(pieces // 2, pieces)) if paired else ()
 
-        def copy(self, lane, block, piece, slot, target):
-            sends, recvs = self.lanes[lane]
-            ref = self.ref.at[block * self.pieces + piece]
+        def remote(self, ref, send_sem, recv_sem, target):
             return pltpu.make_async_remote_copy(
                 src_ref=ref,
                 dst_ref=ref,
-                send_sem=sends.at[slot, piece],
-                recv_sem=recvs.at[slot, piece],
+                send_sem=send_sem,
+                recv_sem=recv_sem,
                 device_id={"tp": target},
                 device_id_type=MESH,
             )
 
-        def hop(self, lane, at, piece, slot):
-            target = {
-                "up": block_of(jnp.minimum(z + 1, line - 1), y),
-                "down": block_of(jnp.maximum(z - 1, 0), y),
-                "across": block_of(z, inner - 1 - y),
-            }[lane]
-            return self.copy(lane, block_of(at, y), piece, slot, target)
-
-        def reach(self, piece, act):
-            for k in range(line - 1, 0, -1):
-                for lane, has, to in (("up", z + k < line, z + k), ("down", z >= k, z - k)):
-                    pl.when(has)(
-                        lambda: act(
-                            self.copy(lane, block_of(z, y), piece, k - 1, block_of(to, y))
-                        )
-                    )
+        def along(self, at, piece, to):
+            return self.remote(
+                self.ref.at[block_of(at, y) * self.pieces + piece],
+                self.column_send.at[0],
+                self.column_recv.at[lax.rem(at - to + line, line) - 1, piece],
+                block_of(to, y),
+            )
+
+        def across(self, at, column, piece, target):
+            return self.remote(
+                self.ref.at[block_of(at, column) * self.pieces + piece],
+                self.across_send.at[0],
+                self.across_recv.at[at, piece // self.half],
+                target,
+            )
 
         def lane_sends(self, lane, k, piece, act):
             up = lane == "up"
             at, has = (z - k, z >= k) if up else (z + k, z + k < line)
-            slot = max(2 * k - 1, 0) if up else 2 * k
-            if k < line - 1 and piece not in self.straight:
-                onward = z + 1 < line if up else z > 0
-                pl.when(has & onward)(lambda: act(self.hop(lane, at, piece, k)))
+            if k < line - 1:
+                onward, to = (z + 1 < line, z + 1) if up else (z > 0, z - 1)
+                pl.when(has & onward)(lambda: act(self.along(at, piece, to)))
             if inner > 1 and (k > 0 or up):
                 if k == 1 and piece in self.turned:
                     has = has & (lax.rem(z, 2) == (0 if up else 1))
-                pl.when(has)(lambda: act(self.hop("across", at, piece, slot)))
-
-        def sends(self, k, piece, act):
-            if k == 0 and piece in self.straight:
-                self.reach(piece, act)
+                pl.when(has)(
+                    lambda: act(self.across(at, y, piece, block_of(z, inner - 1 - y)))
+                )
+
+        def start(self, piece):
             for lane in ("up", "down"):
-                self.lane_sends(lane, k, piece, act)
-
-        def start(self, piece):
-            self.sends(0, piece, lambda c: c.start())
+                self.lane_sends(lane, 0, piece, lambda c: c.start())
 
         def take(self, lane, k, piece):
             at, has = (z - k, z >= k) if lane == "up" else (z + k, z + k < line)
-            pl.when(has)(lambda: self.hop(lane, at, piece, k - 1).wait_recv())
+            pl.when(has)(lambda: self.along(at, piece, z).wait_recv())
             self.lane_sends(lane, k, piece, lambda c: c.start())
 
         def near(self, k, piece):
@@ -592,50 +585,48 @@
             pl.when(z < line // 2)(lambda: self.take("up", k, piece))
             pl.when(z >= line // 2)(lambda: self.take("down", k, piece))
 
-        def side(self, piece):
-            return self.copy(
-                "side", block_of(z, inner - 1 - y), piece, 0, block_of(mate, y)
+        def side_start(self, when, piece):
+            pl.when(when)(
+                lambda: self.across(z, inner - 1 - y, piece, block_of(mate, y)).start()
             )
 
-        def side_start(self, when, piece):
-            pl.when(when)(lambda: self.side(piece).start())
-
-        def arrive(self, i, piece):
+        def arrive(self, i, half):
             at = level(i)
             block = block_of(at, inner - 1 - y)
-            slot = jnp.where(at < z, 2 * (z - at) - 1, 2 * (at - z))
-
-            def plain():
-                self.copy("across", block, piece, slot, block).wait_recv()
-
-            if i == 0 or piece not in self.turned:
-                plain()
-                return
-            pl.when(at != mate)(plain)
-            pl.when(at == mate)(
-                lambda: self.copy("side", block, piece, 0, block).wait_recv()
-            )
+            self.remote(
+                self.ref.at[pl.ds(block * self.pieces + half * self.half, self.half)],
+                self.across_send.at[0],
+                self.across_recv.at[at, half],
+                block,
+            ).wait_recv()
 
         def drain(self):
-            for piece in range(self.pieces):
-                for k in range(line):
-                    self.sends(k, piece, lambda c: c.wait_send())
-                if piece in self.turned:
-                    self.side(piece).wait_send()
+            def sent(count, sem):
+                self.remote(
+                    self.ref.at[pl.ds(0, count * self.pieces)],
+                    sem.at[0],
+                    self.across_recv.at[0, 0],
+                    block_of(z, inner - 1 - y),
+                ).wait_send()
+
+            if line > 1:
+                pl.when(at_end)(lambda: sent(1, self.column_send))
+            if line > 2:
+                pl.when(jnp.logical_not(at_end))(lambda: sent(line + 1, self.column_send))
+            if inner > 1:
+                sent(line, self.across_send)
 
     def run(events):
         for _, act in sorted(enumerate(events), key=lambda e: (e[1][0], e[0])):
             act[1]()
 
-    xg = Gather(x_all, parts, X_STRAIGHT, gather_sems[:8])
-    hg = Gather(ho_all, hparts, H_STRAIGHT, gather_sems[8:16])
-
-    for copy in own_x[0]:
+    xg = Gather(x_all, parts, gather_sems[:4])
+    hg = Gather(ho_all, hparts, gather_sems[4:])
+
+    own_x[0].wait()
+    xg.start(0)
+    for copy in own_x[1:]:
         copy.wait()
-    xg.start(0)
-    for pair in own_x[1:]:
-        for copy in pair:
-            copy.wait()
 
     ones = jnp.ones((16, width), jnp.bfloat16)
     row_sum = jnp.zeros((16, both), f32)
@@ -649,10 +640,13 @@
     stat_all[me] = jnp.zeros(stat_all.shape[1:], f32)
     stat_all[me, 0:1, 0:both] = row_sum[0:1]
     stat_all[me, 1:2, 0:both] = row_squares[0:1]
-    sa = [
-        send(stat_all.at[me], stat_all.at[me], sa_s.at[d - 1], sa_r.at[d - 1], "tp", d)
-        for d in range(1, n)
-    ]
+    sa = Exchange(
+        "tp",
+        3,
+        lambda d: stat_all.at[me],
+        lambda d: stat_all.at[me],
+        stat_all.at[pl.ds(0, n - 1)],
+    )
     for p in range(1, parts):
         xg.start(p)
 
@@ -668,35 +662,29 @@
     conds = short(conds * lax.logistic(conds))
     for which in range(2):
         mod_own[2 * which : 2 * which + 2, :] = nt(conds, mod_w[which])[0:2]
-    m1 = [
-        send(mod_own, mod_recv.at[d - 1], m1_s.at[d - 1], m1_r.at[d - 1], "sp", d)
-        for d in range(1, s)
-    ]
-
-    def exchange_mods():
-        for copy in m1:
-            copy.wait_recv()
+    m1 = Exchange("sp", 0, lambda d: mod_own, lambda d: mod_recv.at[d - 1], mod_recv)
+    held = {}
+
+    def send_mods():
+        m1.wait_recv()
         total = mod_own[...]
         for d in range(1, s):
             total = total + mod_recv[d - 1]
         mod_all[me] = total
-        return [
-            send(mod_all.at[me], mod_all.at[me], m2_s.at[d - 1], m2_r.at[d - 1], "tp", d)
-            for d in range(1, n)
-        ]
-
-    held = {}
-
-    def send_mods():
-        held["m2"] = exchange_mods()
+        held["m2"] = Exchange(
+            "tp",
+            1,
+            lambda d: mod_all.at[me],
+            lambda d: mod_all.at[me],
+            mod_all.at[pl.ds(0, n - 1)],
+        )
 
     def send_gates():
         gate_load.wait()
         gate_own[...] = nt(conds, mod_w[2])[0:2]
-        held["mg"] = [
-            send(gate_own, gate_recv.at[d - 1], mg_s.at[d - 1], mg_r.at[d - 1], "sp", d)
-            for d in range(1, s)
-        ]
+        held["mg"] = Exchange(
+            "sp", 2, lambda d: gate_own, lambda d: gate_recv.at[d - 1], gate_recv
+        )
 
     def early():
         for copy in small:
@@ -712,8 +700,7 @@
         low_acc[...] = jnp.zeros(low_acc.shape, f32)
 
     def moments():
-        for copy in sa:
-            copy.wait_recv()
+        sa.wait_recv()
         stats = sum(stat_all[b] for b in range(n))
         diagonal = lax.broadcasted_iota(jnp.int32, (both, both), 0) == lax.broadcasted_iota(
             jnp.int32, (both, both), 1
@@ -732,8 +719,7 @@
         held["spread"] = lax.rsqrt(column_of(1) - mean * mean + epsilon)
 
     def wait_mods():
-        for copy in held["m2"]:
-            copy.wait_recv()
+        held["m2"].wait_recv()
         for copy in weights:
             copy.wait()
 
@@ -760,8 +746,8 @@
 
     def other_block(i):
         if i > 0:
-            for p in range(parts):
-                xg.arrive(i, p)
+            for half in range(min(parts, 2)):
+                xg.arrive(i, half)
         project_block(block_of(level(i), inner - 1 - y))
 
     unit, lag, cost = 0.79, 2.0, 0.6
@@ -780,21 +766,20 @@
             if 2 * k < line + line % 2:
                 events.append((arrival(k, p) + 0.005, functools.partial(xg.far, k, p)))
     if inner > 1:
-        for p in range(parts):
-            events.append((arrival(1, p) + 0.03, functools.partial(xg.arrive, 0, p)))
-            if p in xg.turned:
+        for half in range(min(parts, 2)):
+            when = arrival(1, (half + 1) * xg.half - 1)
+            events.append((when + 0.03, functools.partial(xg.arrive, 0, half)))
+        for p in xg.turned:
+            when = arrival(1, parts - 1)
+            events.append((when + 0.04, functools.partial(xg.side_start, at_end, p)))
+            if line > 2:
+                when = arrival(line - 2, parts - 1)
                 events.append(
-                    (arrival(1, p) + 0.04, functools.partial(xg.side_start, at_end, p))
+                    (
+                        when + 0.01,
+                        functools.partial(xg.side_start, jnp.logical_not(at_end), p),
+                    )
                 )
-                if line > 2:
-                    events.append(
-                        (
-                            arrival(line - 2, parts - 1) + 0.01,
-                            functools.partial(
-                                xg.side_start, jnp.logical_not(at_end), p
-                            ),
-                        )
-                    )
     tasks = []
     for i in range(line):
         ready = arrival(i, parts - 1) + 0.02 if i else 0.0
@@ -817,14 +802,20 @@
     ctx_low[own_ctx, :] = jnp.zeros((crows, ctx_low.shape[1]), jnp.bfloat16)
     for i, part in enumerate(terms(low_acc[rows:])):
         ctx_low[own_ctx, i * 2 * DECAY_RANK : (i + 1) * 2 * DECAY_RANK] = part
-    lo = [
-        send(ctx_low.at[own_ctx], ctx_low.at[own_ctx], lo_s.at[d - 1], lo_r.at[d - 1], "sp", d)
-        for d in range(1, s)
-    ]
-    kv = [
-        send(ctx_kv.at[own_ctx], ctx_kv.at[own_ctx], kv_s.at[d - 1], kv_r.at[d - 1], "sp", d)
-        for d in range(1, s)
-    ]
+    lo = Exchange(
+        "sp",
+        5,
+        lambda d: ctx_low.at[own_ctx],
+        lambda d: ctx_low.at[own_ctx],
+        ctx_low.at[pl.ds(0, (s - 1) * crows)],
+    )
+    kv = Exchange(
+        "sp",
+        4,
+        lambda d: ctx_kv.at[own_ctx],
+        lambda d: ctx_kv.at[own_ctx],
+        ctx_kv.at[pl.ds(0, (s - 1) * crows)],
+    )
 
     none = jnp.zeros((DECAY_RANK, hk), jnp.bfloat16)
     up_both = jnp.concatenate(
@@ -849,15 +840,12 @@
     whole = [cum[0][rows - 1 : rows], cum[1][0:1]]
     tot_own[0:1, :] = whole[0]
     tot_own[1:2, :] = whole[1]
-    to = [
-        send(tot_own, tot_recv.at[d - 1], to_s.at[d - 1], to_r.at[d - 1], "sp", d)
-        for d in range(1, s)
-    ]
+    to = Exchange("sp", 6, lambda d: tot_own, lambda d: tot_recv.at[d - 1], tot_recv)
 
     keys = proj[0:rows, hk : 2 * hk].astype(f32)
     per = hparts // heads
     weighted = [short(keys * jnp.exp(whole[e] - cum[e])) for e in range(2)]
-    st = {}
+    st = []
     for h in range(heads):
         for e in range(2):
             state = short(
@@ -869,16 +857,17 @@
             for q in range(per):
                 st_own[e, h * per + q] = state[:, q * hwidth : (q + 1) * hwidth]
         for q in range(h * per, (h + 1) * per):
-            for d in range(1, s):
-                later = lax.rem(sp + d, s) > sp
-                st[q, d] = send(
-                    st_own.at[jnp.where(later, 0, 1), q],
-                    st_recv.at[d - 1, q],
-                    st_s.at[d - 1, q],
-                    st_r.at[d - 1, q],
+            st.append(
+                Exchange(
                     "sp",
-                    d,
+                    7 + q,
+                    lambda d: st_own.at[jnp.where(lax.rem(sp + d, s) > sp, 0, 1), q],
+                    lambda d: st_recv.at[d - 1, q],
+                    st_recv.at[:, q],
+                    7,
+                    False,
                 )
+            )
 
     queries = proj[0:rows, 0:hk].astype(f32) * DK ** (-0.5)
     blocks = rows // BLK
@@ -925,8 +914,7 @@
             lines.append(jnp.concatenate(strip, axis=1) if blocks > 1 else strip[0])
         scores.append(short(jnp.concatenate(lines, axis=0) if blocks > 1 else lines[0]))
 
-    for copy in lo:
-        copy.wait_recv()
+    lo.wait_recv()
     low_parts = [
         ctx_low[:, i * 2 * DECAY_RANK : (i + 1) * 2 * DECAY_RANK] for i in range(3)
     ]
@@ -938,8 +926,17 @@
         end = c[length - 1 : length] if e == 0 else c[0:1]
         ctx_decay.append(jnp.exp(end - c))
 
-    for copy in to:
-        copy.wait_recv()
+    kv.wait_recv()
+    ctx_keys = ctx_kv[:, 0:hk].astype(f32)
+    ctx_weighted = [short(ctx_keys * part) for part in ctx_decay]
+    ctx_states = [
+        [
+            short(tn(w[:, h * DK : (h + 1) * DK], ctx_kv[:, hk + h * dv : hk + (h + 1) * dv]))
+            for w in ctx_weighted
+        ]
+        for h in range(heads)
+    ]
+    to.wait_recv()
     places = {d: lax.rem(sp - d + s, s) for d in range(1, s)}
 
     def passed(low_end, high_end, direction):
@@ -964,19 +961,14 @@
     gate_rows = proj[0:rows, 2 * hk + hv :].astype(f32)
     small_gate = gate_rows * lax.logistic(gate_rows) * gain_v[...]
 
-    for copy in kv:
-        copy.wait_recv()
-    ctx_keys = ctx_kv[:, 0:hk].astype(f32)
-    ctx_weighted = [short(ctx_keys * part) for part in ctx_decay]
     for h in range(heads):
         ch = slice(h * DK, (h + 1) * DK)
         vc = slice(h * dv, (h + 1) * dv)
-        ctx_values = ctx_kv[:, hk + h * dv : hk + (h + 1) * dv]
         local_out[:, vc] = nn(
             jnp.concatenate([scores[h]] + [r[:, ch] for r in ctx_reach], axis=1),
             jnp.concatenate(
                 [proj[0:rows, 2 * hk + h * dv : 2 * hk + (h + 1) * dv]]
-                + [short(tn(w[:, ch], ctx_values)) for w in ctx_weighted],
+                + ctx_states[h],
                 axis=0,
             ),
         )
@@ -988,8 +980,7 @@
         h = q // per
         ch = slice(h * DK, (h + 1) * DK)
         vc = slice(q * hwidth, (q + 1) * hwidth)
-        for d in range(1, s):
-            st[q, d].wait_recv()
+        st[q].wait_recv()
         o = local_out[:, vc] + nn(
             jnp.concatenate([r[:, ch] for r in reach], axis=1),
             jnp.concatenate([st_recv[d - 1, q] for d in range(1, s)], axis=0),
@@ -1003,8 +994,7 @@
 
     def ready_out():
         last.wait()
-        for copy in held["mg"]:
-            copy.wait_recv()
+        held["mg"].wait_recv()
         total_out[...] = jnp.zeros(total_out.shape, f32)
 
     def add_half(block, half):
@@ -1019,8 +1009,7 @@
 
     def add_other(i, half):
         if i > 0:
-            hg.arrive(i, 2 * half)
-            hg.arrive(i, 2 * half + 1)
+            hg.arrive(i, half)
         add_half(block_of(level(i), inner - 1 - y), half)
 
     hop_h = 2.6
@@ -1032,21 +1021,18 @@
             events.append((here(k, q), functools.partial(hg.near, k, q)))
             if 2 * k < line + line % 2:
                 events.append((here(k, q) + 0.5, functools.partial(hg.far, k, q)))
-        if inner > 1:
-            events.append((here(1, q) + 0.02, functools.partial(hg.arrive, 0, q)))
-            if q in hg.turned:
+        if q in hg.turned:
+            when = here(1, hparts - 1) + 0.03
+            events.append((when, functools.partial(hg.side_start, at_end, q)))
+            if line > 2:
+                when = here(line - 2, q) + 0.03
                 events.append(
-                    (here(1, q) + 0.03, functools.partial(hg.side_start, at_end, q))
+                    (when, functools.partial(hg.side_start, jnp.logical_not(at_end), q))
                 )
-                if line > 2:
-                    events.append(
-                        (
-                            here(line - 2, q) + 0.03,
-                            functools.partial(
-                                hg.side_start, jnp.logical_not(at_end), q
-                            ),
-                        )
-                    )
+    if inner > 1:
+        for half in range(2):
+            when = here(1, (half + 1) * hg.half - 1) + 0.02
+            events.append((when, functools.partial(hg.arrive, 0, half)))
     for i in range(line):
         for half in range(hparts // 2):
             when = here(i, 2 * half + 1) + 0.6
@@ -1067,6 +1053,15 @@
         )
     for copy in started:
         copy.wait_send()
+    if s > 1:
+        pltpu.make_async_remote_copy(
+            src_ref=st_recv,
+            dst_ref=st_recv,
+            send_sem=x_send.at[7],
+            recv_sem=x_recv.at[7],
+            device_id={"sp": lax.rem(sp + 1, s)},
+            device_id_type=MESH,
+        ).wait_send()
     xg.drain()
     hg.drain()
 
@@ -1104,7 +1099,6 @@
     stat_width = -(-both // 128) * 128
     bf, f32 = jnp.bfloat16, jnp.float32
     vmem, dma = pltpu.VMEM, pltpu.SemaphoreType.DMA
-    pair = lambda *k: [dma(k), dma(k)]
     scratch = [
         vmem((n * parts, both, 128), bf),
         vmem((both, feats), bf),
@@ -1136,21 +1130,20 @@
         vmem((rows, hv), f32),
         vmem((n * hparts, rows, 128), bf),
         vmem((rows, feats), f32),
-        dma((15 + 2 * parts,)),
+        dma((12,)),
+        dma((8,)),
+        dma((7 + hparts,)),
     ]
-    for counts in ((s - 1,), (n - 1,), (s - 1,), (n - 1,), (s - 1,), (s - 1,), (s - 1,), (s - 1, hparts)):
-        scratch += pair(*counts)
     inner = 2 if n % 2 == 0 else 1
     line = n // inner
     hops = max(line - 1, 1)
     for pieces in (parts, hparts):
-        for count in (hops, hops, 2 * line - 1, 1):
-            scratch += pair(count, pieces)
+        scratch += [dma((1,)), dma((1,)), dma((hops, pieces)), dma((line, min(pieces, 2)))]
     return pl.pallas_call(
         functools.partial(
             layer_kernel, n, s, inner, rows, crows, feats, heads, dv, parts, hparts
         ),
-        out_shape=jax.ShapeDtypeStruct((rows, feats), bf),
+        out_shape=pltpu.VMEM((rows, feats), bf),
         in_specs=[pl.BlockSpec(memory_space=pl.ANY)] * 17,
         out_specs=pl.BlockSpec(memory_space=pltpu.VMEM),
         scratch_shapes=scratch,
@@ -1199,7 +1192,7 @@
         P("tp"),
         P("tp", None),
     )
-    whole_heads = HEADS % mesh.shape["tp"] == 0
+    whole_heads = HEADS == 2 * mesh.shape["tp"]
     return jax.shard_map(
         one_kernel if whole_heads else local, mesh=mesh, in_specs=placed, out_specs=P("sp", "tp"), check_vma=False
     )

time: 48.1 us -> 43.9 us (0.913)
  Pallas kernels: 46.4 us -> 43.1 us
  local copies, waits for them, and re-layouts: 1.57 us -> 0.66 us
    pallas_call x1, Pallas kernels: 46.4 us -> 43.1 us  [one_kernel(): pl.pallas_call(functools.partial(layer_kernel, n, s, inner, rows, crows,...]
    unnamed x1, local copies, waits for them, and re-layouts: 1.57 us -> 0.66 us
where the time goes in v3:
time: 43.9 us; the launch traced here: 43.7 us
  Pallas kernels  43.1 us (98%)
  local copies, waits for them, and re-layouts  0.66 us (2%)
    pallas_call x1, Pallas kernels, one_kernel(): pl.pallas_call(functools.partial(layer_kernel, n, s, inner, rows, crows,...  43.1 us

profile of v3, /device:TPU:0, one launch (start us, length us, event | category | flops | bytes accessed | tf_op | source)
XLA Modules:
  0.0 43.7 jit_solution(4641054581251449024)
XLA Ops:
  0.0 43.1 %layer.1 = bf16[128,512]{1,0:T(8,128)(2,1)S(1)} custom-call(bf16[128,512]{1,0:T(8,128)(2,1)} %latent.1, bf16[16,512]{1,0:T(8,128)(2,1)} %context.1, bf16[8,128]{1,0:T(8,128)(2,1)} %bitcast.9, bf16[8,128]{1,0:T(8,128)(2,1)} %bitcast.10, bf16[512,1024]{1,0:T(8,128)(2,1)} %shift_m.1, bf16[512,1024]{1,0:T(8,128)(2,1)} %scale_m.1, bf16[512,1024]{1,0:T(8,128)(2,1)} %gate_m.1, ...), custom_call_target="tpu_custom_call" | custom-call | tf_op jit(solution)/shard_map/layer/pallas_call | solution.py:1142
  43.1 0.7 %copy.19 = bf16[128,512]{1,0:T(8,128)(2,1)} copy(bf16[128,512]{1,0:T(8,128)(2,1)S(1)} %layer.1) | data formatting | bytes 262144

commit v4 on v3

--- a/solution.py
+++ b/solution.py
@@ -405,6 +405,7 @@
     load_sem,
     x_send,
     x_recv,
+    waves,
     *gather_sems,
 ):
     me = lax.axis_index("tp")
@@ -465,16 +466,44 @@
     ]
     last = load((out_m, out_w), whole=out_w)
 
+    line = n // inner
+    z, y = lax.div(me, inner), lax.rem(me, inner)
+    mate = z + 1 - 2 * lax.rem(z, 2)
+    paired = inner > 1 and line % 2 == 0
+    at_end = (z == 0) | (z == line - 1)
+
+    def block_of(at, column):
+        return at * inner + column
+
     barrier = pltpu.get_barrier_semaphore()
-    for d in range(1, n):
+
+    def greet(**where):
+        pl.semaphore_signal(barrier, inc=1, device_id=where, device_id_type=MESH)
+
+    pl.when(z + 1 < line)(lambda: greet(tp=block_of(z + 1, y)))
+    pl.when(z > 0)(lambda: greet(tp=block_of(z - 1, y)))
+    if inner > 1:
+        greet(tp=block_of(z, inner - 1 - y))
+    for d in range(1, s):
+        greet(sp=lax.rem(sp + d, s))
+    beside = jnp.where(z > 0, 1, 0) + jnp.where(z + 1 < line, 1, 0)
+    pl.semaphore_wait(barrier, beside + (inner - 1) + (s - 1))
+
+    def pass_on(way):
         pl.semaphore_signal(
-            barrier, inc=1, device_id={"tp": lax.rem(me + d, n)}, device_id_type=MESH
-        )
-    for d in range(1, s):
-        pl.semaphore_signal(
-            barrier, inc=1, device_id={"sp": lax.rem(sp + d, s)}, device_id_type=MESH
-        )
-    pl.semaphore_wait(barrier, n - 1 + s - 1)
+            waves.at[way],
+            inc=1,
+            device_id={"tp": block_of(z + 1 - 2 * way, y)},
+            device_id_type=MESH,
+        )
+
+    def relay(way):
+        pl.semaphore_wait(waves.at[way], 1)
+        pass_on(way)
+
+    if line > 1:
+        pl.when(z == 0)(lambda: pass_on(0))
+        pl.when(z == line - 1)(lambda: pass_on(1))
 
     started = []
 
@@ -504,12 +533,6 @@
             if self.some:
                 self.all.wait_recv()
 
-    line = n // inner
-    z, y = lax.div(me, inner), lax.rem(me, inner)
-    mate = z + 1 - 2 * lax.rem(z, 2)
-    paired = inner > 1 and line % 2 == 0
-    at_end = (z == 0) | (z == line - 1)
-
     def level(i):
         table = []
         for at in range(line):
@@ -518,9 +541,6 @@
                 order += [b for b in (at - k, at + k) if 0 <= b < line]
             table.append(order[i])
         return sum(jnp.where(z == at, table[at], 0) for at in range(line))
-
-    def block_of(at, column):
-        return at * inner + column
 
     class Gather:
         def __init__(self, ref, pieces, sems):
@@ -623,10 +643,27 @@
     xg = Gather(x_all, parts, gather_sems[:4])
     hg = Gather(ho_all, hparts, gather_sems[4:])
 
-    own_x[0].wait()
-    xg.start(0)
-    for copy in own_x[1:]:
-        copy.wait()
+    for p in range(parts):
+        if p < 2:
+            own_x[p].wait()
+        xg.start(p)
+    if line > 2:
+        pl.when((z > 0) & (z < line - 1))(lambda: relay(0))
+        pl.when(z == line - 2)(lambda: relay(1))
+
+    first[0].wait()
+
+    def one_row(which):
+        part = cond_v[which].astype(f32)
+        return jnp.concatenate([part[r : r + 1] for r in range(part.shape[0])], axis=1)
+
+    row_of = lax.broadcasted_iota(jnp.int32, (16, shift_m.shape[1]), 0)
+    conds = jnp.where(row_of == 0, one_row(0), one_row(1))
+    conds = short(conds * lax.logistic(conds))
+    first[1].wait()
+    for which in range(2):
+        mod_own[2 * which : 2 * which + 2, :] = nt(conds, mod_w[which])[0:2]
+    m1 = Exchange("sp", 0, lambda d: mod_own, lambda d: mod_recv.at[d - 1], mod_recv)
 
     ones = jnp.ones((16, width), jnp.bfloat16)
     row_sum = jnp.zeros((16, both), f32)
@@ -640,30 +677,22 @@
     stat_all[me] = jnp.zeros(stat_all.shape[1:], f32)
     stat_all[me, 0:1, 0:both] = row_sum[0:1]
     stat_all[me, 1:2, 0:both] = row_squares[0:1]
-    sa = Exchange(
-        "tp",
-        3,
-        lambda d: stat_all.at[me],
-        lambda d: stat_all.at[me],
-        stat_all.at[pl.ds(0, n - 1)],
-    )
-    for p in range(1, parts):
-        xg.start(p)
-
-    for copy in first:
-        copy.wait()
-
-    def one_row(which):
-        part = cond_v[which].astype(f32)
-        return jnp.concatenate([part[r : r + 1] for r in range(part.shape[0])], axis=1)
-
-    row_of = lax.broadcasted_iota(jnp.int32, (16, shift_m.shape[1]), 0)
-    conds = jnp.where(row_of == 0, one_row(0), one_row(1))
-    conds = short(conds * lax.logistic(conds))
-    for which in range(2):
-        mod_own[2 * which : 2 * which + 2, :] = nt(conds, mod_w[which])[0:2]
-    m1 = Exchange("sp", 0, lambda d: mod_own, lambda d: mod_recv.at[d - 1], mod_recv)
+
     held = {}
+
+    def send_stats():
+        if line > 1:
+            pl.when(z == line - 1)(lambda: pl.semaphore_wait(waves.at[0], 1))
+            pl.when(z == 0)(lambda: pl.semaphore_wait(waves.at[1], 1))
+        if line > 2:
+            pl.when((z > 0) & (z < line - 2))(lambda: relay(1))
+        held["sa"] = Exchange(
+            "tp",
+            3,
+            lambda d: stat_all.at[me],
+            lambda d: stat_all.at[me],
+            stat_all.at[pl.ds(0, n - 1)],
+        )
 
     def send_mods():
         m1.wait_recv()
@@ -700,7 +729,7 @@
         low_acc[...] = jnp.zeros(low_acc.shape, f32)
 
     def moments():
-        sa.wait_recv()
+        held["sa"].wait_recv()
         stats = sum(stat_all[b] for b in range(n))
         diagonal = lax.broadcasted_iota(jnp.int32, (both, both), 0) == lax.broadcasted_iota(
             jnp.int32, (both, both), 1
@@ -754,6 +783,7 @@
     arrival = lambda k, p: unit * ((k - 1) * parts + p + 1) + lag
     mods_at = 9.4
     events = [
+        (arrival(1, 0) - 0.1, send_stats),
         (arrival(1, parts // 2 - 1) + 0.01, send_mods),
         (arrival(1, parts // 2 - 1) + 0.02, send_gates),
         (arrival(1, parts - 1) + 0.05, early),
@@ -762,9 +792,8 @@
     ]
     for k in range(1, line):
         for p in range(parts):
-            events.append((arrival(k, p), functools.partial(xg.near, k, p)))
-            if 2 * k < line + line % 2:
-                events.append((arrival(k, p) + 0.005, functools.partial(xg.far, k, p)))
+            events.append((arrival(k, p), functools.partial(xg.take, "up", k, p)))
+            events.append((arrival(k, p) + 0.005, functools.partial(xg.take, "down", k, p)))
     if inner > 1:
         for half in range(min(parts, 2)):
             when = arrival(1, (half + 1) * xg.half - 1)
@@ -1133,6 +1162,7 @@
         dma((12,)),
         dma((8,)),
         dma((7 + hparts,)),
+        pltpu.SemaphoreType.REGULAR((2,)),
     ]
     inner = 2 if n % 2 == 0 else 1
     line = n // inner

time: 43.9 us -> 43.2 us (0.984)
  Pallas kernels: 43.1 us -> 42.4 us
    pallas_call x1, Pallas kernels: 43.1 us -> 42.4 us  [one_kernel(): pl.pallas_call(functools.partial(layer_kernel, n, s, inner, rows, crows,...]
where the time goes in v4:
time: 43.2 us; the launch traced here: 43.1 us
  Pallas kernels  42.4 us (98%)
  local copies, waits for them, and re-layouts  0.66 us (2%)
    pallas_call x1, Pallas kernels, one_kernel(): pl.pallas_call(functools.partial(layer_kernel, n, s, inner, rows, crows,...  42.4 us

profile of v4, /device:TPU:0, one launch (start us, length us, event | category | flops | bytes accessed | tf_op | source)
XLA Modules:
  0.0 43.1 jit_solution(15048471410252716021)
XLA Ops:
  0.0 42.4 %layer.1 = bf16[128,512]{1,0:T(8,128)(2,1)S(1)} custom-call(bf16[128,512]{1,0:T(8,128)(2,1)} %latent.1, bf16[16,512]{1,0:T(8,128)(2,1)} %context.1, bf16[8,128]{1,0:T(8,128)(2,1)} %bitcast.9, bf16[8,128]{1,0:T(8,128)(2,1)} %bitcast.10, bf16[512,1024]{1,0:T(8,128)(2,1)} %shift_m.1, bf16[512,1024]{1,0:T(8,128)(2,1)} %scale_m.1, bf16[512,1024]{1,0:T(8,128)(2,1)} %gate_m.1, ...), custom_call_target="tpu_custom_call" | custom-call | tf_op jit(solution)/shard_map/layer/pallas_call | solution.py:1172
  42.4 0.7 %copy.19 = bf16[128,512]{1,0:T(8,128)(2,1)} copy(bf16[128,512]{1,0:T(8,128)(2,1)S(1)} %layer.1) | data formatting | bytes 262144

commit v5 on v4

--- a/solution.py
+++ b/solution.py
@@ -324,6 +324,9 @@
 
 def short(value):
     return value.astype(jnp.bfloat16)
+
+
+H_CUTS = 2
 
 
 def terms(value):
@@ -641,7 +644,8 @@
             act[1]()
 
     xg = Gather(x_all, parts, gather_sems[:4])
-    hg = Gather(ho_all, hparts, gather_sems[4:])
+    hg = Gather(ho_all, hparts * H_CUTS, gather_sems[4:])
+    strip_rows = rows // H_CUTS
 
     for p in range(parts):
         if p < 2:
@@ -838,13 +842,35 @@
         lambda d: ctx_low.at[own_ctx],
         ctx_low.at[pl.ds(0, (s - 1) * crows)],
     )
-    kv = Exchange(
-        "sp",
-        4,
-        lambda d: ctx_kv.at[own_ctx],
-        lambda d: ctx_kv.at[own_ctx],
-        ctx_kv.at[pl.ds(0, (s - 1) * crows)],
-    )
+    mate_core = sp + 1 - 2 * lax.rem(sp, 2)
+    opposite = lax.rem(sp + 2, s)
+    even = lax.rem(sp, 2) == 0
+    toward_mate = jnp.where(mate_core > sp, 0, 1)
+    toward_opposite = jnp.where(opposite > sp, 0, 1)
+
+    def push(src, dst, send_index, recv_index, target):
+        return pltpu.make_async_remote_copy(
+            src_ref=src,
+            dst_ref=dst,
+            send_sem=x_send.at[send_index],
+            recv_sem=x_recv.at[recv_index],
+            device_id={"sp": target},
+            device_id_type=MESH,
+        )
+
+    def kv_rows(source):
+        return ctx_kv.at[pl.ds(pl.multiple_of(source * crows, crows), crows)]
+
+    push(kv_rows(sp), kv_rows(sp), 4, 4, opposite).start()
+    push(kv_rows(sp), kv_rows(sp), 4, 15, mate_core).start()
+
+    def pass_kv():
+        push(kv_rows(opposite), kv_rows(opposite), 4, 4, opposite).wait_recv()
+        push(kv_rows(opposite), kv_rows(opposite), 4, 15, mate_core).start()
+
+    def wait_kv():
+        rest = ctx_kv.at[pl.ds(0, 2 * crows)]
+        push(rest, rest, 4, 15, mate_core).wait_recv()
 
     none = jnp.zeros((DECAY_RANK, hk), jnp.bfloat16)
     up_both = jnp.concatenate(
@@ -874,7 +900,6 @@
     keys = proj[0:rows, hk : 2 * hk].astype(f32)
     per = hparts // heads
     weighted = [short(keys * jnp.exp(whole[e] - cum[e])) for e in range(2)]
-    st = []
     for h in range(heads):
         for e in range(2):
             state = short(
@@ -886,17 +911,25 @@
             for q in range(per):
                 st_own[e, h * per + q] = state[:, q * hwidth : (q + 1) * hwidth]
         for q in range(h * per, (h + 1) * per):
-            st.append(
-                Exchange(
-                    "sp",
-                    7 + q,
-                    lambda d: st_own.at[jnp.where(lax.rem(sp + d, s) > sp, 0, 1), q],
-                    lambda d: st_recv.at[d - 1, q],
-                    st_recv.at[:, q],
-                    7,
-                    False,
-                )
-            )
+            push(
+                st_own.at[toward_opposite, q], st_recv.at[1, q], 7, 7 + q, opposite
+            ).start()
+            push(
+                st_own.at[toward_mate, q],
+                st_recv.at[jnp.where(even, 0, 2), q],
+                7,
+                11 + q,
+                mate_core,
+            ).start()
+
+    def pass_state(q):
+        mine = st_recv.at[1, q]
+        push(mine, mine, 7, 7 + q, opposite).wait_recv()
+        push(mine, st_recv.at[jnp.where(even, 2, 0), q], 7, 11 + q, mate_core).start()
+
+    def wait_state(q):
+        rest = st_recv.at[pl.ds(0, 2), q]
+        push(rest, rest, 7, 11 + q, mate_core).wait_recv()
 
     queries = proj[0:rows, 0:hk].astype(f32) * DK ** (-0.5)
     blocks = rows // BLK
@@ -944,6 +977,7 @@
         scores.append(short(jnp.concatenate(lines, axis=0) if blocks > 1 else lines[0]))
 
     lo.wait_recv()
+    pass_kv()
     low_parts = [
         ctx_low[:, i * 2 * DECAY_RANK : (i + 1) * 2 * DECAY_RANK] for i in range(3)
     ]
@@ -955,16 +989,6 @@
         end = c[length - 1 : length] if e == 0 else c[0:1]
         ctx_decay.append(jnp.exp(end - c))
 
-    kv.wait_recv()
-    ctx_keys = ctx_kv[:, 0:hk].astype(f32)
-    ctx_weighted = [short(ctx_keys * part) for part in ctx_decay]
-    ctx_states = [
-        [
-            short(tn(w[:, h * DK : (h + 1) * DK], ctx_kv[:, hk + h * dv : hk + (h + 1) * dv]))
-            for w in ctx_weighted
-        ]
-        for h in range(heads)
-    ]
     to.wait_recv()
     places = {d: lax.rem(sp - d + s, s) for d in range(1, s)}
 
@@ -990,6 +1014,17 @@
     gate_rows = proj[0:rows, 2 * hk + hv :].astype(f32)
     small_gate = gate_rows * lax.logistic(gate_rows) * gain_v[...]
 
+    pass_state(0)
+    wait_kv()
+    ctx_keys = ctx_kv[:, 0:hk].astype(f32)
+    ctx_weighted = [short(ctx_keys * part) for part in ctx_decay]
+    ctx_states = [
+        [
+            short(tn(w[:, h * DK : (h + 1) * DK], ctx_kv[:, hk + h * dv : hk + (h + 1) * dv]))
+            for w in ctx_weighted
+        ]
+        for h in range(heads)
+    ]
     for h in range(heads):
         ch = slice(h * DK, (h + 1) * DK)
         vc = slice(h * dv, (h + 1) * dv)
@@ -1009,7 +1044,9 @@
         h = q // per
         ch = slice(h * DK, (h + 1) * DK)
         vc = slice(q * hwidth, (q + 1) * hwidth)
-        st[q].wait_recv()
+        if q + 1 < hparts:
+            pass_state(q + 1)
+        wait_state(q)
         o = local_out[:, vc] + nn(
             jnp.concatenate([r[:, ch] for r in reach], axis=1),
             jnp.concatenate([st_recv[d - 1, q] for d in range(1, s)], axis=0),
@@ -1018,8 +1055,11 @@
         top = short(squares)
         rest = short(squares - top.astype(f32))
         power = (nn(top, group) + nn(rest, group)) * (1.0 / VGROUP)
-        ho_all[me * hparts + q] = short(o * lax.rsqrt(power + epsilon) * small_gate[:, vc])
-        hg.start(q)
+        result = short(o * lax.rsqrt(power + epsilon) * small_gate[:, vc])
+        for r in range(H_CUTS):
+            p = q * H_CUTS + r
+            ho_all[me * hg.pieces + p] = result[r * strip_rows : (r + 1) * strip_rows]
+            hg.start(p)
 
     def ready_out():
         last.wait()
@@ -1028,8 +1068,15 @@
 
     def add_half(block, half):
         cols = pl.ds(pl.multiple_of(block * feats + half * 2 * hwidth, 2 * hwidth), 2 * hwidth)
+        first_piece = block * hg.pieces + 2 * half * H_CUTS
         pair = jnp.concatenate(
-            [ho_all[block * hparts + 2 * half], ho_all[block * hparts + 2 * half + 1]], axis=1
+            [
+                jnp.concatenate(
+                    [ho_all[first_piece + r], ho_all[first_piece + H_CUTS + r]], axis=1
+                )
+                for r in range(H_CUTS)
+            ],
+            axis=0,
         )
         total_out[...] += nt(pair, out_w[:, cols])
 
@@ -1046,21 +1093,24 @@
     events = [(here(0, 1) + 0.01, ready_out)]
     for q in range(hparts):
         events.append((here(0, q), functools.partial(head_piece, q)))
-        for k in range(1, line):
-            events.append((here(k, q), functools.partial(hg.near, k, q)))
-            if 2 * k < line + line % 2:
-                events.append((here(k, q) + 0.5, functools.partial(hg.far, k, q)))
-        if q in hg.turned:
-            when = here(1, hparts - 1) + 0.03
-            events.append((when, functools.partial(hg.side_start, at_end, q)))
-            if line > 2:
-                when = here(line - 2, q) + 0.03
-                events.append(
-                    (when, functools.partial(hg.side_start, jnp.logical_not(at_end), q))
-                )
+        for r in range(H_CUTS):
+            p = q * H_CUTS + r
+            for k in range(1, line):
+                events.append((here(k, q) + 0.01 * r, functools.partial(hg.near, k, p)))
+                if 2 * k < line + line % 2:
+                    when = here(k, q) + 0.5 + 0.01 * r
+                    events.append((when, functools.partial(hg.far, k, p)))
+            if p in hg.turned:
+                when = here(1, hparts - 1) + 0.03
+                events.append((when, functools.partial(hg.side_start, at_end, p)))
+                if line > 2:
+                    when = here(line - 2, hparts - 1) + 0.03
+                    events.append(
+                        (when, functools.partial(hg.side_start, jnp.logical_not(at_end), p))
+                    )
     if inner > 1:
         for half in range(2):
-            when = here(1, (half + 1) * hg.half - 1) + 0.02
+            when = here(1, (half + 1) * hparts // 2 - 1) + 0.02
             events.append((when, functools.partial(hg.arrive, 0, half)))
     for i in range(line):
         for half in range(hparts // 2):
@@ -1068,7 +1118,7 @@
             events.append((when, functools.partial(add_column, i, half)))
             if inner > 1:
                 when += hop_h + 0.1
-                if i == 1 and 2 * half in hg.turned:
+                if i == 1 and 2 * half * H_CUTS in hg.turned:
                     when = max(when, here(line - 1, 2 * half + 1) + 0.4)
                 events.append((when, functools.partial(add_other, i, half)))
     run(events)
@@ -1082,15 +1132,9 @@
         )
     for copy in started:
         copy.wait_send()
-    if s > 1:
-        pltpu.make_async_remote_copy(
-            src_ref=st_recv,
-            dst_ref=st_recv,
-            send_sem=x_send.at[7],
-            recv_sem=x_recv.at[7],
-            device_id={"sp": lax.rem(sp + 1, s)},
-            device_id_type=MESH,
-        ).wait_send()
+    push(st_recv, st_recv, 7, 7, opposite).wait_send()
+    sent_kv = ctx_kv.at[pl.ds(0, (s - 1) * crows)]
+    push(sent_kv, sent_kv, 4, 4, opposite).wait_send()
     xg.drain()
     hg.drain()
 
@@ -1157,17 +1201,17 @@
         vmem((2, hparts, DK, 128), bf),
         vmem((s - 1, hparts, DK, 128), bf),
         vmem((rows, hv), f32),
-        vmem((n * hparts, rows, 128), bf),
+        vmem((n * hparts * H_CUTS, rows // H_CUTS, 128), bf),
         vmem((rows, feats), f32),
         dma((12,)),
         dma((8,)),
-        dma((7 + hparts,)),
+        dma((8 + 2 * hparts,)),
         pltpu.SemaphoreType.REGULAR((2,)),
     ]
     inner = 2 if n % 2 == 0 else 1
     line = n // inner
     hops = max(line - 1, 1)
-    for pieces in (parts, hparts):
+    for pieces in (parts, hparts * H_CUTS):
         scratch += [dma((1,)), dma((1,)), dma((hops, pieces)), dma((line, min(pieces, 2)))]
     return pl.pallas_call(
         functools.partial(
@@ -1222,7 +1266,7 @@
         P("tp"),
         P("tp", None),
     )
-    whole_heads = HEADS == 2 * mesh.shape["tp"]
+    whole_heads = HEADS == 2 * mesh.shape["tp"] and mesh.shape["sp"] == 4
     return jax.shard_map(
         one_kernel if whole_heads else local, mesh=mesh, in_specs=placed, out_specs=P("sp", "tp"), check_vma=False
     )

time: 43.2 us -> 42.1 us (0.975)
  Pallas kernels: 42.4 us -> 41.3 us
    pallas_call x1, Pallas kernels: 42.4 us -> 41.3 us  [one_kernel(): pl.pallas_call(functools.partial(layer_kernel, n, s, inner, rows, crows,...]
where the time goes in v5:
time: 42.1 us; the launch traced here: 42 us
  Pallas kernels  41.3 us (98%)
  local copies, waits for them, and re-layouts  0.66 us (2%)
    pallas_call x1, Pallas kernels, one_kernel(): pl.pallas_call(functools.partial(layer_kernel, n, s, inner, rows, crows,...  41.3 us

profile of v5, /device:TPU:0, one launch (start us, length us, event | category | flops | bytes accessed | tf_op | source)
XLA Modules:
  0.0 42.0 jit_solution(2963772464482506378)
XLA Ops:
  0.0 41.3 %layer.1 = bf16[128,512]{1,0:T(8,128)(2,1)S(1)} custom-call(bf16[128,512]{1,0:T(8,128)(2,1)} %latent.1, bf16[16,512]{1,0:T(8,128)(2,1)} %context.1, bf16[8,128]{1,0:T(8,128)(2,1)} %bitcast.9, bf16[8,128]{1,0:T(8,128)(2,1)} %bitcast.10, bf16[512,1024]{1,0:T(8,128)(2,1)} %shift_m.1, bf16[512,1024]{1,0:T(8,128)(2,1)} %scale_m.1, bf16[512,1024]{1,0:T(8,128)(2,1)} %gate_m.1, ...), custom_call_target="tpu_custom_call" | custom-call | tf_op jit(solution)/shard_map/layer/pallas_call | solution.py:1216
  41.3 0.7 %copy.19 = bf16[128,512]{1,0:T(8,128)(2,1)} copy(bf16[128,512]{1,0:T(8,128)(2,1)S(1)} %layer.1) | data formatting | bytes 262144
